TPU v7x, 256 devices: a whole 4x4x8 slice. The times are simulated.
256 devices in a mesh: ep: 16 (over y, x), tp: 16 (over z, core).
Axes of the slice: x: 4, y: 4, z: 8, core: 2. Of those that a mesh axis runs over, the one named last changes fastest.
Arguments:
- mix_tokens: bfloat16 [4096, 4096], P('ep'), may hold values from -6 to 6
- mix_gain: float32 [4096], replicated, may hold values from 0.1 to 1.9
- value_weight: bfloat16 [4096, 2048], P(None, 'tp'), may hold values from -0.09375 to 0.09375
- inner_weight: bfloat16 [4096, 2048], P(None, 'tp'), may hold values from -0.09375 to 0.09375
- outer_weight: bfloat16 [4096, 2048], P(None, 'tp'), may hold values from -0.09375 to 0.09375
- conv_taps: float32 [3, 2048], P(None, 'tp'), may hold values from -3 to 3
- mix_weight: bfloat16 [2048, 4096], P('tp'), may hold values from -0.125 to 0.125
- moe_tokens: bfloat16 [4096, 4096], P('ep'), may hold values from -6 to 6
- moe_gain: float32 [4096], replicated, may hold values from 0.1 to 1.9
- router_group: bfloat16 [4096, 4], replicated, may hold values from -0.09375 to 0.09375
- router_expert: bfloat16 [4096, 16], replicated, may hold values from -0.09375 to 0.09375
- expert_routes: int32 [4096, 2], P('ep'), may hold values from 0 to 15, as said below
- gate_weight: bfloat16 [16, 4096, 2048], P('ep', None, 'tp'), may hold values from -0.09375 to 0.09375
- up_weight: bfloat16 [16, 4096, 2048], P('ep', None, 'tp'), may hold values from -0.09375 to 0.09375
- down_weight: bfloat16 [16, 2048, 4096], P('ep', 'tp'), may hold values from -0.5 to 0.5
Outputs:
- mixer_out: bfloat16 [4096, 4096], P(('ep', 'tp'))
- expert_out: bfloat16 [4096, 4096], P(('ep', 'tp'))
Inputs may be any that keep to these rules, and one draw needn't show every extreme that they name: `expert_routes`: the two experts of a row are different and lie in one group of 4 consecutive expert numbers. In each aligned block of 16 rows no expert is named more than 4 times, and in every draw some experts are named exactly 4 times in every block.
All inputs are finite; a program needn't handle non-finite values.
Results may differ from a plain program's by a relative error of at most 0.0076.
Values may be sent and summed in bfloat16 or wider, within the bound.
A program may use at most 128 MiB of HBM per device.

v0:
```python
import jax
import jax.numpy as jnp
from jax import lax
from jax.sharding import PartitionSpec as P

TAPS = 3
EXPERTS = 16
GROUPS = 4
TOPK = 2
MOE_SHARE = 16
EPG = 4
CAP = 4


def from_behind(value, axis, steps):
    count = lax.axis_size(axis)
    initial, last = (max(0, -steps), min(count, count - steps))
    return lax.ppermute(value, axis, [(source, source + steps) for source in range(initial, last)])


def rms_rows(inputs, gain_vec):
    values = inputs.astype(jnp.float32)
    inverse = lax.rsqrt(jnp.mean(values * values, axis=-1, keepdims=True) + 1e-06)
    return (values * inverse * gain_vec).astype(jnp.bfloat16)


def route_weights(normed, routes, router_group, router_expert):
    group_logit = jnp.dot(normed, router_group, preferred_element_type=jnp.float32)
    expert_logit = jnp.dot(normed, router_expert, preferred_element_type=jnp.float32)
    group_exp = jnp.exp(group_logit)
    group_id = routes[:, 0] // EPG
    group_pick = (group_id[:, None] == jnp.arange(GROUPS, dtype=jnp.int32)[None, :]).astype(
        jnp.float32
    )
    group_gate = jnp.sum(group_exp * group_pick, axis=1) / jnp.sum(group_exp, axis=1)
    expert_pick = (
        routes[:, :, None] == jnp.arange(EXPERTS, dtype=jnp.int32)[None, None, :]
    ).astype(jnp.float32)
    chosen = jnp.exp(jnp.sum(expert_logit[:, None, :] * expert_pick, axis=2))
    return group_gate[:, None] * chosen / jnp.sum(chosen, axis=1, keepdims=True)


def block_ranks(routes):
    blocks = routes.shape[0]
    entries = routes.reshape(blocks, MOE_SHARE * TOPK)
    one_hot = (entries[:, :, None] == jnp.arange(EXPERTS, dtype=jnp.int32)[None, None, :]).astype(
        jnp.int32
    )
    before = jnp.cumsum(one_hot, axis=1) - one_hot
    return jnp.sum(before * one_hot, axis=2).reshape(routes.shape)


def dispatch_rows(normed, routes):
    slot_ids = routes * CAP + block_ranks(routes)
    targets = jnp.arange(EXPERTS * CAP, dtype=jnp.int32)
    select = (slot_ids[:, None, :, :] == targets[None, :, None, None]).astype(jnp.int32)
    select = jnp.sum(select, axis=3).astype(jnp.bfloat16)
    placed = jnp.einsum("bcs,bsd->bcd", select, normed, preferred_element_type=jnp.float32)
    return placed.astype(jnp.bfloat16).reshape(normed.shape[0], EXPERTS, CAP, normed.shape[2])


def expert_hidden(arrived, gate_weight, up_weight):
    gate_proj = jnp.einsum(
        "besd,edf->besf", arrived, gate_weight, preferred_element_type=jnp.float32
    )
    up_proj = jnp.einsum("besd,edf->besf", arrived, up_weight, preferred_element_type=jnp.float32)
    return (jax.nn.silu(gate_proj) * up_proj).astype(jnp.bfloat16)


def mixer_half(
    mix_tokens, mix_gain, value_weight, inner_weight, outer_weight, conv_taps, mix_weight
):
    normed = rms_rows(mix_tokens, mix_gain)
    value_proj = jnp.dot(normed, value_weight, preferred_element_type=jnp.float32)
    inner_proj = jnp.dot(normed, inner_weight, preferred_element_type=jnp.float32)
    outer_proj = jnp.dot(normed, outer_weight, preferred_element_type=jnp.float32)
    gated_in = (inner_proj * value_proj).astype(jnp.bfloat16)
    earlier = from_behind(gated_in[gated_in.shape[0] - (TAPS - 1) :], "ep", 1)
    padded = jnp.concatenate([earlier, gated_in], axis=0).astype(jnp.float32)
    seq_rows = gated_in.shape[0]
    mixed_conv = conv_taps[0] * padded[0:seq_rows]
    for tap_index in range(1, TAPS):
        mixed_conv = mixed_conv + conv_taps[tap_index] * padded[tap_index : tap_index + seq_rows]
    conv_out = (outer_proj * mixed_conv).astype(jnp.bfloat16)
    summed = lax.psum_scatter(
        jnp.dot(conv_out, mix_weight, preferred_element_type=jnp.float32),
        "tp",
        scatter_dimension=0,
        tiled=True,
    )
    return summed.astype(jnp.bfloat16)


def local(
    mix_tokens,
    mix_gain,
    value_weight,
    inner_weight,
    outer_weight,
    conv_taps,
    mix_weight,
    moe_tokens,
    moe_gain,
    router_group,
    router_expert,
    expert_routes,
    gate_weight,
    up_weight,
    down_weight,
):
    mixer_out = mixer_half(
        mix_tokens, mix_gain, value_weight, inner_weight, outer_weight, conv_taps, mix_weight
    )
    tp_index = lax.axis_index("tp")
    model_width = moe_tokens.shape[1]
    own_routes = lax.dynamic_slice_in_dim(expert_routes, tp_index * MOE_SHARE, MOE_SHARE, 0)
    own_tokens = lax.dynamic_slice_in_dim(moe_tokens, tp_index * MOE_SHARE, MOE_SHARE, 0)
    own_normed = rms_rows(own_tokens, moe_gain)
    placed = dispatch_rows(own_normed[None], own_routes[None])[0]
    arrived = lax.all_to_all(placed, "ep", split_axis=0, concat_axis=1, tiled=True)
    hidden = expert_hidden(
        lax.all_gather(arrived[None], "tp", axis=0, tiled=True), gate_weight, up_weight
    )
    local_experts = hidden.shape[1]
    slot_count = hidden.shape[2]
    per_block = local_experts * slot_count
    partial_value = jnp.einsum(
        "besf,efd->besd", hidden, down_weight, preferred_element_type=jnp.float32
    )
    summed = lax.psum_scatter(
        partial_value.reshape(per_block * lax.axis_size("tp"), model_width),
        "tp",
        scatter_dimension=0,
        tiled=True,
    )
    results = summed.astype(jnp.bfloat16).reshape(
        local_experts, slot_count // CAP, CAP, model_width
    )
    returned = lax.all_to_all(results, "ep", split_axis=1, concat_axis=0, tiled=True).reshape(
        EXPERTS * CAP, model_width
    )
    weights = route_weights(own_normed, own_routes, router_group, router_expert)
    own_slots = own_routes * CAP + block_ranks(own_routes[None])[0]
    picked = jnp.take(returned, own_slots, axis=0).astype(jnp.float32)
    expert_out = jnp.sum(weights[:, :, None] * picked, axis=1).astype(jnp.bfloat16)
    return (mixer_out, expert_out)


def solution(mesh):
    return jax.shard_map(
        local,
        mesh=mesh,
        in_specs=(
            P("ep", None),
            P(),
            P(None, "tp"),
            P(None, "tp"),
            P(None, "tp"),
            P(None, "tp"),
            P("tp", None),
            P("ep", None),
            P(),
            P(),
            P(),
            P("ep", None),
            P("ep", None, "tp"),
            P("ep", None, "tp"),
            P("ep", "tp", None),
        ),
        out_specs=(P(("ep", "tp"), None), P(("ep", "tp"), None)),
        check_vma=False,
    )
```

profile of v0, /device:TPU:3, one launch (start us, length us, event | category | flops | bytes accessed | tf_op | source)
XLA Modules:
  0.0 278.6 jit_solution(8360812834643250856)
XLA Ops:
  7.2 0.8 constant_dynamic-slice_fusion
  8.4 0.2 select_reduce_fusion
  8.7 0.8 compare_and_fusion
  9.6 1.0 fusion.37
  10.6 1.3 convolution_convert_fusion
  11.9 0.2 squeeze_reshape.7
  12.1 16.1 %all_to_all.8 = bf16[16,4,4096]{2,1,0:T(4,128)(2,1)S(1)} all-to-all(bf16[16,4,4096]{2,1,0:T(4,128)(2,1)S(1)} %squeeze_reshape.7), channel_id=1, replica_groups=mesh['ep'=16,'tp'=16] {'ep'}, dimensions={0} | all-to-all | bytes 1048576 | tf_op jit(solution)/shard_map/all_to_all | solution.py:120
  28.2 0.9 broadcast_in_dim.12
  29.2 57.7 %all-gather.2.cloned.1.call-done = bf16[16,1,64,4096]{3,2,1,0:T(8,128)(2,1)} async-done(((bf16[1,1,64,4096]{3,2,1,0:T(8,128)(2,1)}), bf16[16,1,64,4096]{3,2,1,0:T(8,128)(2,1)}) %all-gather.2.cloned.1.call-update) | async-done | bytes 8388624 | tf_op jit(solution)/shard_map/all_gather | solution.py:122
  86.9 5.9 %fusion.7 = f32[16,1,64,128]{3,2,0,1:T(8,128)S(1)} fusion(bf16[16,1,64,4096]{3,2,1,0:T(8,128)(2,1)} %all-gather.2.cloned.1.call-done, bf16[1,4096,128]{2,1,0:T(8,128)(2,1)} %param.27), kind=kOutput, calls=%fused_computation.11 | convolution fusion | flops 1073741824 | bytes 9961472 | tf_op jit(solution)/shard_map/besd,edf->besf/dot_general | solution.py:63
  92.8 14.4 %fusion.23 = f32[16,64,4096]{2,1,0:T(8,128)} fusion(bf16[16,1,64,4096]{3,2,1,0:T(8,128)(2,1)} %all-gather.2.cloned.1.call-done, bf16[1,128,4096]{2,1,0:T(8,128)(2,1)S(1)} %copy-done, bf16[1,4096,128]{2,1,0:T(8,128)(2,1)S(1)} %copy-done.2, f32[16,1,64,128]{3,2,0,1:T(8,128)S(1)} %fusion.7), kind=kOutput, calls=%fused_computation.16 | convolution fusion | flops 2148270080 | bytes 27787264 | tf_op jit(solution)/shard_map/besf,efd->besd/dot_general | solution.py:127
  107.3 1.5 copy-done.1
  108.8 0.5 fusion.4
  109.3 2.1 fusion.57
  111.4 0.9 fusion.26
  112.3 3.1 %collective-permute-start = (bf16[2,128]{1,0:T(2,128)(2,1)S(1)}, bf16[2,128]{1,0:T(2,128)(2,1)S(1)}, u32[]{:S(2)}, u32[]{:S(2)}) collective-permute-start(bf16[2,128]{1,0:T(2,128)(2,1)S(1)} %slice.34), channel_id=1, source_target_pairs={{0,16},{16,32},{32,48},{48,64},{64,80},{80,96},{96,112},{112,128},... | collective-permute-start | bytes 1544 | tf_op jit(solution)/shard_map/ppermute | solution.py:18
  115.4 1.2 collective-permute-done
  116.6 5.3 %fusion.27 = f32[256,4096]{1,0:T(8,128)} fusion(bf16[128,4096]{1,0:T(8,128)(2,1)} %param.21, bf16[4096,128]{1,0:T(8,128)(2,1)} %param.19, f32[258,128]{1,0:T(8,128)S(1)} %maximum_convert_fusion, f32[128]{0:T(128)S(1)} %get-tuple-element.7, f32[128]{0:T(128)S(1)} %get-tuple-element.8, f32[128]{0:T(128)S(1)} %get-tuple-element.6, ...), kind=kOutput, calls=%fused_computation.21 | convolution fusion | flops 541294592 | bytes 8800768 | tf_op jit(solution)/shard_map/dot_general | solution.py:86
  122.0 0.7 copy-done.4
  122.7 1.1 fusion.61
  123.9 1.1 fusion.53
  125.1 80.0 %reduce-scatter.5.cloned.1.call-done = f32[64,4096]{1,0:T(8,128)} async-done(((f32[1024,4096]{1,0:T(8,128)}), f32[64,4096]{1,0:T(8,128)}) %reduce-scatter.5.cloned.1.call-update) | async-done | bytes 1048592 | tf_op jit(solution)/shard_map/reduce_scatter | solution.py:130
  205.0 1.3 convert_element_type.92
  206.3 1.0 reshape.229
  207.3 6.7 %all-to-all-start.1 = ((bf16[1,16,4,4096]{3,2,0,1:T(4,128)(2,1)}), bf16[1,16,4,4096]{3,2,0,1:T(4,128)(2,1)S(1)}, u32[]{:S(2)}, u32[]{:S(2)}) async-start(bf16[1,16,4,4096]{3,2,0,1:T(4,128)(2,1)} %reshape.229), calls=%async_computation.3 | async-start | bytes 1048576 | tf_op jit(solution)/shard_map/all_to_all | solution.py:139
  214.0 0.2 select_reduce_fusion.1
  214.6 53.3 %reduce-scatter.3.cloned.1.call-done = f32[16,4096]{1,0:T(8,128)} async-done(((f32[256,4096]{1,0:T(8,128)}), f32[16,4096]{1,0:T(8,128)}) %reduce-scatter.3.cloned.1.call-update) | async-done | bytes 262160 | tf_op jit(solution)/shard_map/reduce_scatter | solution.py:85
  267.9 1.6 convert_element_type.84
  269.5 0.1 reshape.230
  269.7 0.7 gather_fusion
  270.4 0.2 reshape.232
  270.6 1.5 multiply_reduce_fusion
  (45 shorter events, 1.3 us)
Async XLA Ops:
  7.2 85.7 %copy-start = (bf16[1,128,4096]{2,1,0:T(8,128)(2,1)S(1)}, bf16[1,128,4096]{2,1,0:T(8,128)(2,1)}, u32[]{:S(2)}) copy-start(bf16[1,128,4096]{2,1,0:T(8,128)(2,1)} %param.29) | copy-start | bytes 3145732
  7.2 79.7 %all-gather.2.cloned.1.call-start = ((), (), s32[]{:S(2)}) async-start(), calls=%async_computation.5 | async-start | bytes 8912896 | tf_op jit(solution)/shard_map/all_gather | solution.py:122
  29.1 63.7 %copy-start.2 = (bf16[1,4096,128]{2,1,0:T(8,128)(2,1)S(1)}, bf16[1,4096,128]{2,1,0:T(8,128)(2,1)}, u32[]{:S(2)}) copy-start(bf16[1,4096,128]{2,1,0:T(8,128)(2,1)} %param.28) | copy-start | bytes 3145732
  29.1 175.9 %reduce-scatter.5.cloned.1.call-start = ((), (), s32[]{:S(2)}) async-start(), calls=%async_computation.6 | async-start | bytes 17825792 | tf_op jit(solution)/shard_map/reduce_scatter | solution.py:130
  107.2 1.6 copy-start.1
  107.2 2.1 copy-start.3
  107.2 160.7 %reduce-scatter.3.cloned.1.call-start = ((), (), s32[]{:S(2)}) async-start(), calls=%async_computation.4 | async-start | bytes 4456448 | tf_op jit(solution)/shard_map/reduce_scatter | solution.py:85
  108.8 2.6 copy-start.6
  109.3 6.1 %copy-start.5 = (f32[3,128]{1,0:T(4,128)S(1)}, f32[3,128]{1,0:T(4,128)}, u32[]{:S(2)}) copy-start(f32[3,128]{1,0:T(4,128)} %param.20) | copy-start | bytes 4612
  112.3 4.3 %collective-permute-start = (bf16[2,128]{1,0:T(2,128)(2,1)S(1)}, bf16[2,128]{1,0:T(2,128)(2,1)S(1)}, u32[]{:S(2)}, u32[]{:S(2)}) collective-permute-start(bf16[2,128]{1,0:T(2,128)(2,1)S(1)} %slice.34), channel_id=1, source_target_pairs={{0,16},{16,32},{32,48},{48,64},{64,80},{80,96},{96,112},{112,128},... | collective-permute-start | bytes 1544 | tf_op jit(solution)/shard_map/ppermute | solution.py:18
  122.0 0.7 copy-start.4
  122.0 0.8 copy-start.8
  122.0 1.9 copy-start.7
  207.3 62.2 %all-to-all-start.1 = ((bf16[1,16,4,4096]{3,2,0,1:T(4,128)(2,1)}), bf16[1,16,4,4096]{3,2,0,1:T(4,128)(2,1)S(1)}, u32[]{:S(2)}, u32[]{:S(2)}) async-start(bf16[1,16,4,4096]{3,2,0,1:T(4,128)(2,1)} %reshape.229), calls=%async_computation.3 | async-start | bytes 1048576 | tf_op jit(solution)/shard_map/all_to_all | solution.py:139
Sparse Core Ops, SparseCore 0:
  29.2 57.6 all-gather.1
  107.4 97.6 reduce-scatter.4
  207.6 60.2 reduce-scatter.2
where the time goes:
time: 282 us; the launch traced here: 279 us
  waiting for transfers between devices  192 us (68%)
  matrix products  32.1 us (11%)
  blocking collectives  16.1 us (6%)
  between operations  14 us (5%)
  starting transfers between devices  9.93 us (4%)
  other arithmetic  7.33 us (3%)
  local copies, waits for them, and re-layouts  6.92 us (2%)
    reduce_scatter x1, waiting for transfers between devices, local(): lax.psum_scatter(partial_value.reshape(per_block * lax.axis_size('tp'), m...  80 us
    all_gather x1, waiting for transfers between devices, local(): lax.all_gather(arrived[None], 'tp', axis=0, tiled=True)  57.7 us
    reduce_scatter x1, waiting for transfers between devices, mixer_half(): lax.psum_scatter(jnp.dot(conv_out, mix_weight, preferred_element_type=jnp...  53.3 us
    all_to_all x1, blocking collectives, local(): lax.all_to_all(placed, 'ep', split_axis=0, concat_axis=1, tiled=True)  16.1 us
    dot_general x1, matrix products, local(): jnp.einsum('besf,efd->besd', hidden, down_weight, preferred_element_type=...  14.4 us
    all_to_all x1, starting transfers between devices, local(): lax.all_to_all(results, 'ep', split_axis=1, concat_axis=0, tiled=True)  6.71 us
    dot_general x1, matrix products, expert_hidden(): jnp.einsum('besd,edf->besf', arrived, gate_weight, preferred_element_type...  5.93 us
  transfers between devices with their start and end apart: 5, of which 4 were waited for; matrix products, arithmetic and copies ran while one was open for 6% of the time, Pallas kernels for 0%

commit v1 on v0

v1 whole, which is shorter than its diff:
```python
import functools

import jax
import jax.numpy as jnp
from jax import lax
from jax.experimental import pallas as pl
from jax.experimental.pallas import tpu as pltpu
from jax.sharding import PartitionSpec as P

MESH = pl.DeviceIdType.MESH
F32 = jnp.float32
BF16 = jnp.bfloat16
SHARE = 16
CAP = 4
EPG = 4
EPS = 1e-06
PIECES = 4


def rms_into(raw, gain_ref, out):
    gain = gain_ref[...]

    def body(i, carry):
        rows = pl.ds(pl.multiple_of(i * SHARE, SHARE), SHARE)
        values = raw[rows, :].astype(F32)
        inverse = lax.rsqrt(jnp.mean(values * values, axis=-1, keepdims=True) + EPS)
        out[rows, :] = (values * inverse * gain).astype(BF16)
        return carry

    lax.fori_loop(0, raw.shape[0] // SHARE, body, 0)


def kernel(
    EP,
    Z,
    mix_x,
    mix_gain,
    value_w,
    inner_w,
    outer_w,
    taps,
    mix_w,
    moe_x,
    moe_gain,
    router_g,
    router_e,
    routes,
    gate_w,
    up_w,
    down_w,
    mix_out,
    moe_out,
    raw_m,
    raw_e,
    norm_m,
    norm_e,
    gu_w,
    dn_w,
    proj_w,
    mixw,
    select,
    select_all,
    send,
    recv,
    acc,
    rs_send,
    rs_recv,
    halo_out,
    halo_in,
    gated,
    outer_p,
    conv,
    conv_all,
    mix_part,
    comb_w,
    ret_send,
    ret_recv,
    comb,
    comb_in,
    load_sem,
    swap_send,
    swap_recv,
    disp_send,
    disp_recv,
    hop_send,
    hop_recv,
    halo_sem,
    conv_sem,
    back_send,
    back_recv,
    last_send,
    last_recv,
):
    tokens, width = raw_m.shape
    C = value_w.shape[1]
    F = gate_w.shape[1]
    half = EP // 2
    rows = half * 2 * CAP
    piece = width // PIECES
    hops = Z // 2

    e = lax.axis_index("ep")
    tp = lax.axis_index("tp")
    z, c = tp // 2, lax.rem(tp, 2)
    ep_odd = lax.rem(e, 2)
    slot = e // 2
    partner = (e, z * 2 + 1 - c)

    def to_expert(i):
        return (2 * i + c, z * 2 + 1 - ep_odd)

    def to_source(i):
        return (2 * i + 1 - c, z * 2 + ep_odd)

    def beside(step):
        return (e, lax.rem(z + step + Z, Z) * 2 + c)

    def remote(src, dst, ssem, rsem, device):
        return pltpu.make_async_remote_copy(
            src_ref=src, dst_ref=dst, send_sem=ssem, recv_sem=rsem, device_id=device, device_id_type=MESH
        )

    loads = [
        pltpu.make_async_copy(src, dst, load_sem.at[n])
        for n, (src, dst) in enumerate(
            [
                (moe_x, raw_e),
                (mix_x, raw_m),
                (value_w, proj_w.at[:, 0:C]),
                (inner_w, proj_w.at[:, C : 2 * C]),
                (outer_w, proj_w.at[:, 2 * C : 3 * C]),
                (mix_w, mixw.at[0:C]),
                (gate_w, gu_w.at[:, 0:F]),
                (up_w, gu_w.at[:, 2 * F : 3 * F]),
                (down_w, dn_w.at[0:F]),
            ]
        )
    ]
    for copy in loads:
        copy.start()

    barrier = pltpu.get_barrier_semaphore()
    greet = [to_expert(i) for i in range(half)] + [to_source(i) for i in range(half)]
    greet += [beside(1), beside(-1)]
    greet += [(lax.rem(e + 1, EP), tp), (lax.rem(e + EP - 1, EP), tp)]
    for device in greet:
        pl.semaphore_signal(barrier, inc=1, device_id=device, device_id_type=MESH)

    r0 = routes[0:1, :]
    r1 = routes[1:2, :]
    row = lax.broadcasted_iota(jnp.int32, (rows, tokens), 0)
    tok = lax.broadcasted_iota(jnp.int32, (rows, tokens), 1)
    expert_of = 2 * (row >> 3) + c
    named = (r0 == expert_of) | (r1 == expert_of)
    before_r = lax.broadcasted_iota(jnp.int32, (tokens, tokens), 0)
    before_c = lax.broadcasted_iota(jnp.int32, (tokens, tokens), 1)
    before = ((before_r < before_c) & ((before_r >> 4) == (before_c >> 4))).astype(F32).astype(BF16)
    rank = jnp.dot(named.astype(F32).astype(BF16), before, preferred_element_type=F32)
    hit = named & (rank == (row & 3).astype(F32)) & (((tok >> 4) & 1) == ((row >> 2) & 1))
    hit = hit.astype(F32)
    select[...] = hit

    def home_of(s):
        k = (s + 1) // 2
        sign = 2 * lax.rem(s, 2) - 1
        return lax.rem(z + jnp.where(s == 0, hops, sign * (hops - k)) + Z, Z)

    def stage_select(s):
        t = lax.broadcasted_iota(jnp.int32, (rows, tokens), 1)
        return jnp.where((t >> 5) == home_of(s), select[...], 0.0).astype(BF16)

    loads[0].wait()
    rms_into(raw_e, moe_gain, norm_e)
    first = stage_select(jnp.int32(0))

    def place_first(n, carry):
        cols = pl.ds(pl.multiple_of(n * 512, 512), 512)
        placed = jnp.dot(first, norm_e[:, cols], preferred_element_type=F32)
        send[0, :, :, cols] = placed.reshape(half, 2 * CAP, 512).astype(BF16)
        return carry

    lax.fori_loop(0, width // 512, place_first, 0)

    pl.semaphore_wait(barrier, len(greet))

    def dispatch(s):
        for i in range(half):
            remote(send.at[s, i], recv.at[s, slot], disp_send.at[s], disp_recv.at[s], to_expert(i)).start()

    dispatch(0)
    swaps = [
        remote(src, dst, swap_send.at[n], swap_recv.at[n], partner)
        for n, (src, dst) in enumerate(
            [
                (gate_w, gu_w.at[:, F : 2 * F]),
                (up_w, gu_w.at[:, 3 * F : 4 * F]),
                (mix_w, mixw.at[C : 2 * C]),
                (down_w, dn_w.at[F : 2 * F]),
            ]
        )
    ]
    for copy in swaps:
        copy.start()

    for s in range(1, Z):
        select_all[(s - 1) * rows : s * rows, :] = stage_select(jnp.int32(s))

    def place_rest(n, carry):
        cols = pl.ds(pl.multiple_of(n * 256, 256), 256)
        placed = jnp.dot(select_all[...], norm_e[:, cols], preferred_element_type=F32)
        send[pl.ds(1, Z - 1), :, :, cols] = placed.reshape(Z - 1, half, 2 * CAP, 256).astype(BF16)
        return carry

    lax.fori_loop(0, width // 256, place_rest, 0)

    def dispatch_rest(s, carry):
        dispatch(s)
        return carry

    lax.fori_loop(1, Z, dispatch_rest, 0)

    loads[1].wait()
    rms_into(raw_m, mix_gain, norm_m)
    for n in (2, 3, 4):
        loads[n].wait()
    proj = jnp.dot(norm_m[...], proj_w[...], preferred_element_type=F32)
    gated_in = (proj[:, C : 2 * C] * proj[:, 0:C]).astype(BF16)
    outer_p[...] = proj[:, 2 * C : 3 * C]
    gated[pl.ds(SHARE, tokens), :] = gated_in.astype(F32)
    halo_out[...] = gated_in[tokens - SHARE :, :]
    halo = remote(halo_out, halo_in, halo_sem.at[0], halo_sem.at[1], (lax.rem(e + 1, EP), tp))
    halo.start()

    home = 2 * SHARE
    pick_r = lax.broadcasted_iota(jnp.int32, (tokens, home), 0)
    pick_c = lax.broadcasted_iota(jnp.int32, (tokens, home), 1)
    pick = (pick_r == pick_c + z * home).astype(F32).astype(BF16)
    own = jnp.dot(routes[...].astype(F32).astype(BF16), pick, preferred_element_type=F32)
    h0, h1 = own[0:1, :], own[1:2, :]
    own_normed = norm_e[pl.ds(pl.multiple_of(z * home, home), home), :]
    contract_last = (((1,), (1,)), ((), ()))
    group_logit = lax.dot_general(router_g[...], own_normed, contract_last, preferred_element_type=F32)
    expert_logit = lax.dot_general(router_e[...], own_normed, contract_last, preferred_element_type=F32)
    group_exp = jnp.exp(group_logit)
    first_of = (lax.broadcasted_iota(jnp.int32, group_exp.shape, 0) * EPG).astype(F32)
    in_group = (h0 >= first_of) & (h0 < first_of + EPG)
    gate = jnp.sum(jnp.where(in_group, group_exp, 0.0), axis=0, keepdims=True) / jnp.sum(
        group_exp, axis=0, keepdims=True
    )
    number = lax.broadcasted_iota(jnp.int32, expert_logit.shape, 0).astype(F32)
    chosen0 = jnp.exp(jnp.sum(jnp.where(number == h0, expert_logit, 0.0), axis=0, keepdims=True))
    chosen1 = jnp.exp(jnp.sum(jnp.where(number == h1, expert_logit, 0.0), axis=0, keepdims=True))
    both = chosen0 + chosen1
    w0, w1 = gate * chosen0 / both, gate * chosen1 / both
    row_h = lax.broadcasted_iota(jnp.int32, (rows, home), 0)
    tok_h = lax.broadcasted_iota(jnp.int32, (rows, home), 1)
    expert_h = (2 * (row_h >> 3) + c).astype(F32)
    is0, is1 = h0 == expert_h, h1 == expert_h
    bef_r = lax.broadcasted_iota(jnp.int32, (home, home), 0)
    bef_c = lax.broadcasted_iota(jnp.int32, (home, home), 1)
    bef = ((bef_r < bef_c) & ((bef_r >> 4) == (bef_c >> 4))).astype(F32).astype(BF16)
    rank_h = jnp.dot((is0 | is1).astype(F32).astype(BF16), bef, preferred_element_type=F32)
    at = (rank_h == (row_h & 3).astype(F32)) & ((tok_h >> 4) == ((row_h >> 2) & 1))
    weight = jnp.where(at & is0, w0, 0.0) + jnp.where(at & is1, w1, 0.0)
    weight = weight.T
    high = weight.astype(BF16)
    comb_w[0:home, :] = high
    comb_w[home : 2 * home, :] = (weight - high.astype(F32)).astype(BF16)

    halo.wait()
    gated[0:SHARE, :] = jnp.where(e > 0, halo_in[...].astype(F32), 0.0)
    mixed = taps[0:1, :] * gated[pl.ds(SHARE - 2, tokens), :]
    mixed = mixed + taps[1:2, :] * gated[pl.ds(SHARE - 1, tokens), :]
    mixed = mixed + taps[2:3, :] * gated[pl.ds(SHARE, tokens), :]
    conv_out = (outer_p[...] * mixed).astype(BF16).reshape(Z, 2, SHARE, C)
    conv[0] = conv_out[:, 0].reshape(Z * SHARE, C)
    conv[1] = conv_out[:, 1].reshape(Z * SHARE, C)
    conv_swap = remote(conv.at[1 - c], conv_all.at[:, C : 2 * C], conv_sem.at[0], conv_sem.at[1], partner)
    conv_swap.start()
    conv_all[:, 0:C] = conv[c]
    loads[5].wait()
    swaps[2].wait_recv()
    conv_swap.wait()

    def down_mix(n, carry):
        cols = pl.ds(pl.multiple_of(n * 512, 512), 512)
        part = jnp.dot(conv_all[...], mixw[:, cols], preferred_element_type=F32)
        mix_part[:, :, cols] = part.reshape(Z, SHARE, 512)
        return carry

    lax.fori_loop(0, width // 512, down_mix, 0)
    for n in (6, 7, 8):
        loads[n].wait()
    for n in (0, 1, 3):
        swaps[n].wait_recv()

    def hop(direction, k, j):
        return remote(
            rs_send.at[direction, k, j],
            rs_recv.at[direction, k, j],
            hop_send.at[direction, k, j],
            hop_recv.at[direction, k, j],
            beside(2 * direction - 1),
        )

    def give_back(j, i):
        return remote(ret_send.at[j, i], ret_recv.at[j, slot], back_send.at[j], back_recv.at[j], to_source(i))

    def stage(s, carry):
        arrived = remote(send.at[s], recv.at[s], disp_send.at[s], disp_recv.at[s], partner)
        arrived.wait_recv()
        x = recv[s].reshape(rows, width)
        gate_up = jnp.dot(x, gu_w[...], preferred_element_type=F32)
        g, u = gate_up[:, 0 : 2 * F], gate_up[:, 2 * F :]
        hidden = (g / (1.0 + jnp.exp(-g)) * u).astype(BF16)
        direction = lax.rem(s, 2)
        k = (s + 1) // 2
        zs = home_of(s)
        for j in range(PIECES):
            cols = slice(j * piece, (j + 1) * piece)
            side = 1 if j < PIECES // 2 else 0
            acc[0:rows, :] = jnp.dot(hidden, dn_w[:, cols], preferred_element_type=F32)
            acc[rows:, :] = mix_part[zs, :, cols]

            @pl.when(s == 0)
            def _():
                rs_send[side, 0, j] = acc[...].astype(BF16)
                hop(side, 0, j).start()

            @pl.when((s > 0) & (s < Z - 1))
            def _():
                @pl.when((k > 1) | (direction == side))
                def _():
                    hop(direction, k - 1, j).wait_recv()
                    acc[...] += rs_recv[direction, k - 1, j].astype(F32)

                rs_send[direction, k, j] = acc[...].astype(BF16)
                hop(direction, k, j).start()

            @pl.when(s == Z - 1)
            def _():
                for way in (1, 0):
                    hop(way, hops - 1, j).wait_recv()
                    acc[...] += rs_recv[way, hops - 1, j].astype(F32)
                ret_send[j] = acc[0:rows, :].astype(BF16).reshape(half, 2 * CAP, piece)
                for i in range(half):
                    give_back(j, i).start()
                mix_out[:, cols] = acc[rows:, :].astype(BF16)

        return carry

    lax.fori_loop(0, Z, stage, 0)

    def last(j):
        return remote(comb.at[j, 1 - c], comb_in.at[j], last_send.at[j], last_recv.at[j], partner)

    for j in range(PIECES):
        remote(ret_send.at[j], ret_recv.at[j], back_send.at[j], back_recv.at[j], partner).wait_recv()
        summed = jnp.dot(comb_w[...], ret_recv[j].reshape(rows, piece), preferred_element_type=F32)
        comb[j] = (summed[0:home] + summed[home:]).reshape(2, SHARE, piece)
        last(j).start()
    for j in range(PIECES):
        last(j).wait_recv()
        moe_out[:, j * piece : (j + 1) * piece] = (comb[j, c] + comb_in[j]).astype(BF16)

    for copy in swaps:
        copy.wait_send()
    for s in range(Z):
        remote(send.at[s], recv.at[s], disp_send.at[s], disp_recv.at[s], partner).wait_send()
    for j in range(PIECES):
        hop(1 if j < PIECES // 2 else 0, 0, j).wait_send()
        for k in range(1, hops):
            for direction in (0, 1):
                hop(direction, k, j).wait_send()
        remote(ret_send.at[j], ret_recv.at[j], back_send.at[j], back_recv.at[j], partner).wait_send()
        last(j).wait_send()


def solution(mesh):
    EP, TP = mesh.shape["ep"], mesh.shape["tp"]
    Z = TP // 2

    def local(
        mix_tokens,
        mix_gain,
        value_weight,
        inner_weight,
        outer_weight,
        conv_taps,
        mix_weight,
        moe_tokens,
        moe_gain,
        router_group,
        router_expert,
        expert_routes,
        gate_weight,
        up_weight,
        down_weight,
    ):
        tokens, D = mix_tokens.shape
        C = value_weight.shape[1]
        F = gate_weight.shape[2]
        half = EP // 2
        rows = half * 2 * CAP
        piece = D // PIECES
        hops = Z // 2
        vmem = pl.BlockSpec(memory_space=pltpu.VMEM)
        hbm = pl.BlockSpec(memory_space=pl.ANY)
        V = pltpu.VMEM
        DMA = pltpu.SemaphoreType.DMA
        out = jax.ShapeDtypeStruct((SHARE, D), BF16)
        return pl.pallas_call(
            functools.partial(kernel, EP, Z),
            out_shape=(out, out),
            in_specs=[hbm, vmem, hbm, hbm, hbm, vmem, hbm, hbm, vmem, vmem, vmem, vmem, hbm, hbm, hbm],
            out_specs=(vmem, vmem),
            scratch_shapes=[
                V((tokens, D), BF16),
                V((tokens, D), BF16),
                V((tokens, D), BF16),
                V((tokens, D), BF16),
                V((D, 4 * F), BF16),
                V((2 * F, D), BF16),
                V((D, 3 * C), BF16),
                V((2 * C, D), BF16),
                V((rows, tokens), F32),
                V(((Z - 1) * rows, tokens), BF16),
                V((Z, half, 2 * CAP, D), BF16),
                V((Z, half, 2 * CAP, D), BF16),
                V((rows + SHARE, piece), F32),
                V((2, hops, PIECES, rows + SHARE, piece), BF16),
                V((2, hops, PIECES, rows + SHARE, piece), BF16),
                V((SHARE, C), BF16),
                V((SHARE, C), BF16),
                V((SHARE + tokens, C), F32),
                V((tokens, C), F32),
                V((2, Z * SHARE, C), BF16),
                V((Z * SHARE, 2 * C), BF16),
                V((Z, SHARE, D), F32),
                V((4 * SHARE, rows), BF16),
                V((PIECES, half, 2 * CAP, piece), BF16),
                V((PIECES, half, 2 * CAP, piece), BF16),
                V((PIECES, 2, SHARE, piece), F32),
                V((PIECES, SHARE, piece), F32),
                DMA((9,)),
                DMA((4,)),
                DMA((4,)),
                DMA((Z,)),
                DMA((Z,)),
                DMA((2, hops, PIECES)),
                DMA((2, hops, PIECES)),
                DMA((2,)),
                DMA((2,)),
                DMA((PIECES,)),
                DMA((PIECES,)),
                DMA((PIECES,)),
                DMA((PIECES,)),
            ],
            compiler_params=pltpu.CompilerParams(
                collective_id=0, has_side_effects=True, vmem_limit_bytes=60 * 1024 * 1024
            ),
            name="mixer_and_experts",
        )(
            mix_tokens,
            mix_gain.reshape(1, D),
            value_weight,
            inner_weight,
            outer_weight,
            conv_taps,
            mix_weight,
            moe_tokens,
            moe_gain.reshape(1, D),
            router_group.T,
            router_expert.T,
            expert_routes.T,
            gate_weight.reshape(D, F),
            up_weight.reshape(D, F),
            down_weight.reshape(F, D),
        )

    return jax.shard_map(
        local,
        mesh=mesh,
        in_specs=(
            P("ep", None),
            P(),
            P(None, "tp"),
            P(None, "tp"),
            P(None, "tp"),
            P(None, "tp"),
            P("tp", None),
            P("ep", None),
            P(),
            P(),
            P(),
            P("ep", None),
            P("ep", None, "tp"),
            P("ep", None, "tp"),
            P("ep", "tp", None),
        ),
        out_specs=(P(("ep", "tp"), None), P(("ep", "tp"), None)),
        check_vma=False,
    )
```

time: 282 us -> 128 us (0.45); the launches traced: 279 us -> 128 us
  waiting for transfers between devices: 192 us -> 0 us
  Pallas kernels: 0 us -> 125 us
  matrix products: 32.1 us -> 0 us
  blocking collectives: 16.1 us -> 0 us
  between operations: 14 us -> 0.64 us
  starting transfers between devices: 9.93 us -> 0 us
  other arithmetic: 7.33 us -> 0 us
  local copies, waits for them, and re-layouts: 6.92 us -> 3.14 us
    reduce_scatter x2 -> x0, waiting for transfers between devices: 133 us -> none  [the longest x1 80 us: local(): lax.psum_scatter(partial_value.reshape(per_block * lax.axis_size('tp'), m...]
    pallas_call x0 -> x1, Pallas kernels: none -> 125 us  [local(): pl.pallas_call(functools.partial(kernel, EP, Z), out_shape=(out, out), in...]
    all_gather x1 -> x0, waiting for transfers between devices: 57.7 us -> none  [local(): lax.all_gather(arrived[None], 'tp', axis=0, tiled=True)]
    dot_general x8 -> x0, matrix products: 32.1 us -> none  [the longest x1 14.4 us: local(): jnp.einsum('besf,efd->besd', hidden, down_weight, preferred_element_type=...]
    all_to_all x1 -> x0, blocking collectives: 16.1 us -> none  [local(): lax.all_to_all(placed, 'ep', split_axis=0, concat_axis=1, tiled=True)]
    all_to_all x1 -> x0, starting transfers between devices: 6.71 us -> none  [local(): lax.all_to_all(results, 'ep', split_axis=1, concat_axis=0, tiled=True)]
    reduce_sum x7 -> x0, other arithmetic: 3.46 us -> none  [the longest x2 1.54 us: rms_rows(): jnp.mean(values * values, axis=-1, keepdims=True) + 1e-06]
    ppermute x1 -> x0, starting transfers between devices: 3.09 us -> none  [from_behind(): lax.ppermute(value, axis, [(source, source + steps) for source in range(i...]
  transfers between devices with their start and end apart: 5 -> 0, of which waited for: 4 -> 0; matrix products, arithmetic and copies ran while one was open for 6% -> 0% of each run, Pallas kernels for 0% -> 0%
where the time goes in v1:
time: 128 us
  Pallas kernels  125 us (98%)
  local copies, waits for them, and re-layouts  3.14 us (2%)
    pallas_call x1, Pallas kernels, local(): pl.pallas_call(functools.partial(kernel, EP, Z), out_shape=(out, out), in...  125 us
    unnamed x2, local copies, waits for them, and re-layouts  3.14 us

profile of v1, /device:TPU:3, one launch (start us, length us, event | category | flops | bytes accessed | tf_op | source)
XLA Modules:
  0.0 128.3 jit_solution(4860945367822195045)
XLA Ops:
  0.6 124.5 %mixer_and_experts.1 = (bf16[16,4096]{1,0:T(8,128)(2,1)}, bf16[16,4096]{1,0:T(8,128)(2,1)}) custom-call(bf16[256,4096]{1,0:T(8,128)(2,1)} %mix_x.1, f32[1,4096]{1,0:T(1,128)} %bitcast.13, bf16[4096,128]{1,0:T(8,128)(2,1)} %value_w.1, bf16[4096,128]{1,0:T(8,128)(2,1)} %inner_w.1, bf16[4096,128]{1,0:T(8,128)(2,1)} %outer_w.1, f32[3,128]{1,0:T(4,128)} %taps.1, ...), custom_call_target="tpu_custom_call" | custom-call | tf_op jit(solution)/shard_map/mixer_and_experts/pallas_call | solution.py:412
  125.2 1.6 %copy.19 = bf16[16,4096]{1,0:T(8,128)(2,1)} copy(bf16[16,4096]{1,0:T(8,128)(2,1)} %get-tuple-element.4) | data formatting | bytes 262144
  126.7 1.6 %copy.20 = bf16[16,4096]{1,0:T(8,128)(2,1)} copy(bf16[16,4096]{1,0:T(8,128)(2,1)} %get-tuple-element.5) | data formatting | bytes 262144

commit v2 on v1

v2 whole, which is shorter than its diff:
```python
import functools

import jax
import jax.numpy as jnp
from jax import lax
from jax.experimental import pallas as pl
from jax.experimental.pallas import tpu as pltpu
from jax.sharding import PartitionSpec as P

MESH = pl.DeviceIdType.MESH
F32 = jnp.float32
BF16 = jnp.bfloat16
SHARE = 16
CAP = 4
EPG = 4
EPS = 1e-06
PIECES = 4
AHEAD = 3


def rms_rows(raw, gain, out, start, count):
    def body(i, carry):
        rows = pl.ds(pl.multiple_of(start + i * SHARE, SHARE), SHARE)
        values = raw[rows, :].astype(F32)
        inverse = lax.rsqrt(jnp.mean(values * values, axis=-1, keepdims=True) + EPS)
        out[rows, :] = (values * inverse * gain).astype(BF16)
        return carry

    lax.fori_loop(0, count // SHARE, body, 0)


def kernel(
    EP,
    Z,
    mix_x,
    mix_gain,
    value_w,
    inner_w,
    outer_w,
    taps,
    mix_w,
    moe_x,
    moe_gain,
    router_g,
    router_e,
    routes,
    gate_w,
    up_w,
    down_w,
    mix_out,
    moe_out,
    raw_m,
    raw_e,
    norm_m,
    norm_e,
    gu_w,
    dn_w,
    proj_w,
    mixw,
    send,
    recv,
    acc,
    rs_send,
    rs_recv,
    halo_out,
    halo_in,
    gated,
    outer_p,
    conv,
    conv_all,
    mix_part,
    comb_w,
    ret_send,
    ret_recv,
    comb,
    comb_in,
    load_sem,
    tok_sem,
    swap_send,
    swap_recv,
    disp_send,
    disp_recv,
    hop_send,
    hop_recv,
    first_send,
    first_recv,
    halo_sem,
    conv_sem,
    back_send,
    back_recv,
    last_send,
    last_recv,
):
    tokens, width = raw_m.shape
    C = value_w.shape[1]
    F = gate_w.shape[1]
    half = EP // 2
    rows = half * 2 * CAP
    piece = width // PIECES
    hops = Z // 2

    e = lax.axis_index("ep")
    tp = lax.axis_index("tp")
    z, c = tp // 2, lax.rem(tp, 2)
    ep_odd = lax.rem(e, 2)
    slot = e // 2
    partner = (e, z * 2 + 1 - c)

    def to_expert(i):
        return (2 * i + c, z * 2 + 1 - ep_odd)

    def to_source(i):
        return (2 * i + 1 - c, z * 2 + ep_odd)

    def beside(step):
        return (e, lax.rem(z + step + Z, Z) * 2 + c)

    def remote(src, dst, ssem, rsem, device):
        return pltpu.make_async_remote_copy(
            src_ref=src, dst_ref=dst, send_sem=ssem, recv_sem=rsem, device_id=device, device_id_type=MESH
        )

    home = 2 * SHARE

    def home_of(s):
        k = (s + 1) // 2
        sign = 2 * lax.rem(s, 2) - 1
        return lax.rem(z + jnp.where(s == 0, hops, sign * (hops - k)) + Z, Z)

    def token_load(s):
        span = pl.ds(pl.multiple_of(home_of(s) * home, home), home)
        return pltpu.make_async_copy(moe_x.at[span], raw_e.at[span], tok_sem.at[s])

    token_load(0).start()
    loads = [
        pltpu.make_async_copy(src, dst, load_sem.at[n])
        for n, (src, dst) in enumerate(
            [
                (mix_x, raw_m),
                (value_w, proj_w.at[:, 0:C]),
                (inner_w, proj_w.at[:, C : 2 * C]),
                (outer_w, proj_w.at[:, 2 * C : 3 * C]),
                (mix_w, mixw.at[0:C]),
                (gate_w, gu_w.at[:, 0:F]),
                (up_w, gu_w.at[:, 2 * F : 3 * F]),
                (down_w, dn_w.at[0:F]),
            ]
        )
    ]
    barrier = pltpu.get_barrier_semaphore()
    greet = [to_expert(i) for i in range(half)] + [to_source(i) for i in range(half)]
    greet += [beside(1), beside(-1)]
    greet += [(lax.rem(e + 1, EP), tp), (lax.rem(e + EP - 1, EP), tp)]
    for device in greet:
        pl.semaphore_signal(barrier, inc=1, device_id=device, device_id_type=MESH)
    for copy in loads[0:4]:
        copy.start()

    def load_tokens(s, carry):
        token_load(s).start()
        return carry

    lax.fori_loop(1, Z, load_tokens, 0)
    for copy in loads[4:]:
        copy.start()

    row = lax.broadcasted_iota(jnp.int32, (rows, home), 0)
    tok = lax.broadcasted_iota(jnp.int32, (rows, home), 1)
    expert_of = (2 * (row >> 3) + c).astype(F32)
    slot_of = (row & 3).astype(F32)
    in_block = (tok >> 4) == ((row >> 2) & 1)
    bef_r = lax.broadcasted_iota(jnp.int32, (home, home), 0)
    bef_c = lax.broadcasted_iota(jnp.int32, (home, home), 1)
    before = ((bef_r < bef_c) & ((bef_r >> 4) == (bef_c >> 4))).astype(F32).astype(BF16)
    pick_r = lax.broadcasted_iota(jnp.int32, (tokens, home), 0)
    pick_c = lax.broadcasted_iota(jnp.int32, (tokens, home), 1)
    routes_b = routes[...].astype(F32).astype(BF16)

    def routed(zh):
        pick = (pick_r == pick_c + zh * home).astype(F32).astype(BF16)
        named = jnp.dot(routes_b, pick, preferred_element_type=F32)
        h0, h1 = named[0:1, :], named[1:2, :]
        is0, is1 = h0 == expert_of, h1 == expert_of
        rank = jnp.dot((is0 | is1).astype(F32).astype(BF16), before, preferred_element_type=F32)
        at = (rank == slot_of) & in_block
        return h0, h1, at & is0, at & is1

    def dispatch(s):
        for i in range(half):
            remote(send.at[s, i], recv.at[s, slot], disp_send.at[s], disp_recv.at[s], to_expert(i)).start()

    def place(s):
        zh = home_of(s)
        _, _, at0, at1 = routed(zh)
        chosen = (at0 | at1).astype(F32).astype(BF16)
        start = pl.multiple_of(zh * home, home)
        token_load(s).wait()
        rms_rows(raw_e, moe_gain[...], norm_e, start, home)

        def columns(n, carry):
            cols = pl.ds(pl.multiple_of(n * 512, 512), 512)
            placed = jnp.dot(chosen, norm_e[pl.ds(start, home), cols], preferred_element_type=F32)
            send[s, :, :, cols] = placed.reshape(half, 2 * CAP, 512).astype(BF16)
            return carry

        lax.fori_loop(0, width // 512, columns, 0)

        @pl.when(s == 0)
        def _():
            pl.semaphore_wait(barrier, len(greet))

        dispatch(s)

    swaps = [
        remote(src, dst, swap_send.at[n], swap_recv.at[n], partner)
        for n, (src, dst) in enumerate(
            [
                (gate_w, gu_w.at[:, F : 2 * F]),
                (up_w, gu_w.at[:, 3 * F : 4 * F]),
                (mix_w, mixw.at[C : 2 * C]),
                (down_w, dn_w.at[F : 2 * F]),
            ]
        )
    ]
    halo = remote(halo_out, halo_in, halo_sem.at[0], halo_sem.at[1], (lax.rem(e + 1, EP), tp))
    conv_swap = remote(conv.at[1 - c], conv_all.at[:, C : 2 * C], conv_sem.at[0], conv_sem.at[1], partner)

    def mixer_head():
        loads[0].wait()
        rms_rows(raw_m, mix_gain[...], norm_m, 0, tokens)
        for n in (1, 2, 3):
            loads[n].wait()
        proj = jnp.dot(norm_m[...], proj_w[...], preferred_element_type=F32)
        gated_in = (proj[:, C : 2 * C] * proj[:, 0:C]).astype(BF16)
        outer_p[...] = proj[:, 2 * C : 3 * C]
        gated[pl.ds(SHARE, tokens), :] = gated_in.astype(F32)
        halo_out[...] = gated_in[tokens - SHARE :, :]
        halo.start()

    def mixer_conv():
        halo.wait()
        gated[0:SHARE, :] = jnp.where(e > 0, halo_in[...].astype(F32), 0.0)
        mixed = taps[0:1, :] * gated[pl.ds(SHARE - 2, tokens), :]
        mixed = mixed + taps[1:2, :] * gated[pl.ds(SHARE - 1, tokens), :]
        mixed = mixed + taps[2:3, :] * gated[pl.ds(SHARE, tokens), :]
        conv_out = (outer_p[...] * mixed).astype(BF16).reshape(Z, 2, SHARE, C)
        conv[0] = conv_out[:, 0].reshape(Z * SHARE, C)
        conv[1] = conv_out[:, 1].reshape(Z * SHARE, C)
        conv_swap.start()
        conv_all[:, 0:C] = conv[c]

    def first_mix(j):
        side = 1 if j < PIECES // 2 else 0
        return remote(
            rs_send.at[side, 0, j, rows:],
            rs_recv.at[side, 0, j, rows:],
            first_send.at[j],
            first_recv.at[j],
            beside(2 * side - 1),
        )

    def mixer_down():
        loads[4].wait()
        swaps[2].wait_recv()
        conv_swap.wait()

        def down_mix(n, carry):
            cols = pl.ds(pl.multiple_of(n * 512, 512), 512)
            part = jnp.dot(conv_all[...], mixw[:, cols], preferred_element_type=F32)
            mix_part[:, :, cols] = part.reshape(Z, SHARE, 512)
            return carry

        lax.fori_loop(0, width // 512, down_mix, 0)
        far = home_of(0)
        for j in range(PIECES):
            side = 1 if j < PIECES // 2 else 0
            rs_send[side, 0, j, rows:, :] = mix_part[far, :, j * piece : (j + 1) * piece].astype(BF16)
            first_mix(j).start()

    def weigh():
        h0, h1, at0, at1 = routed(z)
        own_normed = norm_e[pl.ds(pl.multiple_of(z * home, home), home), :]
        contract_last = (((1,), (1,)), ((), ()))
        group_logit = lax.dot_general(router_g[...], own_normed, contract_last, preferred_element_type=F32)
        expert_logit = lax.dot_general(router_e[...], own_normed, contract_last, preferred_element_type=F32)
        group_exp = jnp.exp(group_logit)
        first_of = (lax.broadcasted_iota(jnp.int32, group_exp.shape, 0) * EPG).astype(F32)
        in_group = (h0 >= first_of) & (h0 < first_of + EPG)
        gate = jnp.sum(jnp.where(in_group, group_exp, 0.0), axis=0, keepdims=True) / jnp.sum(
            group_exp, axis=0, keepdims=True
        )
        number = lax.broadcasted_iota(jnp.int32, expert_logit.shape, 0).astype(F32)
        chosen0 = jnp.exp(jnp.sum(jnp.where(number == h0, expert_logit, 0.0), axis=0, keepdims=True))
        chosen1 = jnp.exp(jnp.sum(jnp.where(number == h1, expert_logit, 0.0), axis=0, keepdims=True))
        both = chosen0 + chosen1
        weight = jnp.where(at0, gate * chosen0 / both, 0.0) + jnp.where(at1, gate * chosen1 / both, 0.0)
        weight = weight.T
        high = weight.astype(BF16)
        comb_w[0:home, :] = high
        comb_w[home : 2 * home, :] = (weight - high.astype(F32)).astype(BF16)

    def hop(direction, k, j):
        return remote(
            rs_send.at[direction, k, j],
            rs_recv.at[direction, k, j],
            hop_send.at[direction, k, j],
            hop_recv.at[direction, k, j],
            beside(2 * direction - 1),
        )

    def give_back(j, i):
        return remote(ret_send.at[j, i], ret_recv.at[j, slot], back_send.at[j], back_recv.at[j], to_source(i))

    def first_rows(j):
        side = 1 if j < PIECES // 2 else 0
        return remote(
            rs_send.at[side, 0, j, 0:rows],
            rs_recv.at[side, 0, j, 0:rows],
            hop_send.at[side, 0, j],
            hop_recv.at[side, 0, j],
            beside(2 * side - 1),
        )

    def stage(s, carry):
        @pl.when(s + AHEAD < Z)
        def _():
            place(s + AHEAD)

        @pl.when(s == 0)
        def _():
            mixer_conv()
            for n in (5, 6, 7):
                loads[n].wait()
            for n in (0, 1, 3):
                swaps[n].wait_recv()

        @pl.when(s == 1)
        def _():
            mixer_down()

        @pl.when(s == Z - AHEAD)
        def _():
            weigh()

        arrived = remote(send.at[s], recv.at[s], disp_send.at[s], disp_recv.at[s], partner)
        arrived.wait_recv()
        x = recv[s].reshape(rows, width)
        gate_up = jnp.dot(x, gu_w[...], preferred_element_type=F32)
        g, u = gate_up[:, 0 : 2 * F], gate_up[:, 2 * F :]
        hidden = (g / (1.0 + jnp.exp(-g)) * u).astype(BF16)
        direction = lax.rem(s, 2)
        k = (s + 1) // 2
        zs = home_of(s)
        for j in range(PIECES):
            cols = slice(j * piece, (j + 1) * piece)
            side = 1 if j < PIECES // 2 else 0
            acc[0:rows, :] = jnp.dot(hidden, dn_w[:, cols], preferred_element_type=F32)

            @pl.when(s == 0)
            def _():
                rs_send[side, 0, j, 0:rows, :] = acc[0:rows, :].astype(BF16)
                first_rows(j).start()

            @pl.when((s > 0) & (s < Z - 1))
            def _():
                acc[rows:, :] = mix_part[zs, :, cols]

                @pl.when((k == 1) & (direction == side))
                def _():
                    first_rows(j).wait_recv()
                    first_mix(j).wait_recv()
                    acc[...] += rs_recv[side, 0, j].astype(F32)

                @pl.when(k > 1)
                def _():
                    hop(direction, k - 1, j).wait_recv()
                    acc[...] += rs_recv[direction, k - 1, j].astype(F32)

                rs_send[direction, k, j] = acc[...].astype(BF16)
                hop(direction, k, j).start()

            @pl.when(s == Z - 1)
            def _():
                acc[rows:, :] = mix_part[zs, :, cols]
                for way in (1, 0):
                    hop(way, hops - 1, j).wait_recv()
                    acc[...] += rs_recv[way, hops - 1, j].astype(F32)
                ret_send[j] = acc[0:rows, :].astype(BF16).reshape(half, 2 * CAP, piece)
                for i in range(half):
                    give_back(j, i).start()
                mix_out[:, cols] = acc[rows:, :].astype(BF16)

        return carry

    place(jnp.int32(0))
    for copy in swaps:
        copy.start()
    mixer_head()

    def place_early(s, carry):
        place(s)
        return carry

    lax.fori_loop(1, AHEAD, place_early, 0)
    lax.fori_loop(0, Z, stage, 0)

    def last(j):
        return remote(comb.at[j, 1 - c], comb_in.at[j], last_send.at[j], last_recv.at[j], partner)

    for j in range(PIECES):
        remote(ret_send.at[j], ret_recv.at[j], back_send.at[j], back_recv.at[j], partner).wait_recv()
        summed = jnp.dot(comb_w[...], ret_recv[j].reshape(rows, piece), preferred_element_type=F32)
        comb[j] = (summed[0:home] + summed[home:]).reshape(2, SHARE, piece)
        last(j).start()
    for j in range(PIECES):
        last(j).wait_recv()
        moe_out[:, j * piece : (j + 1) * piece] = (comb[j, c] + comb_in[j]).astype(BF16)

    for copy in swaps:
        copy.wait_send()
    for s in range(Z):
        remote(send.at[s], recv.at[s], disp_send.at[s], disp_recv.at[s], partner).wait_send()
    for j in range(PIECES):
        first_rows(j).wait_send()
        first_mix(j).wait_send()
        for k in range(1, hops):
            for direction in (0, 1):
                hop(direction, k, j).wait_send()
        remote(ret_send.at[j], ret_recv.at[j], back_send.at[j], back_recv.at[j], partner).wait_send()
        last(j).wait_send()


def solution(mesh):
    EP, TP = mesh.shape["ep"], mesh.shape["tp"]
    Z = TP // 2

    def local(
        mix_tokens,
        mix_gain,
        value_weight,
        inner_weight,
        outer_weight,
        conv_taps,
        mix_weight,
        moe_tokens,
        moe_gain,
        router_group,
        router_expert,
        expert_routes,
        gate_weight,
        up_weight,
        down_weight,
    ):
        tokens, D = mix_tokens.shape
        C = value_weight.shape[1]
        F = gate_weight.shape[2]
        half = EP // 2
        rows = half * 2 * CAP
        piece = D // PIECES
        hops = Z // 2
        vmem = pl.BlockSpec(memory_space=pltpu.VMEM)
        hbm = pl.BlockSpec(memory_space=pl.ANY)
        V = pltpu.VMEM
        DMA = pltpu.SemaphoreType.DMA
        out = jax.ShapeDtypeStruct((SHARE, D), BF16)
        return pl.pallas_call(
            functools.partial(kernel, EP, Z),
            out_shape=(out, out),
            in_specs=[hbm, vmem, hbm, hbm, hbm, vmem, hbm, hbm, vmem, vmem, vmem, vmem, hbm, hbm, hbm],
            out_specs=(vmem, vmem),
            scratch_shapes=[
                V((tokens, D), BF16),
                V((tokens, D), BF16),
                V((tokens, D), BF16),
                V((tokens, D), BF16),
                V((D, 4 * F), BF16),
                V((2 * F, D), BF16),
                V((D, 3 * C), BF16),
                V((2 * C, D), BF16),
                V((Z, half, 2 * CAP, D), BF16),
                V((Z, half, 2 * CAP, D), BF16),
                V((rows + SHARE, piece), F32),
                V((2, hops, PIECES, rows + SHARE, piece), BF16),
                V((2, hops, PIECES, rows + SHARE, piece), BF16),
                V((SHARE, C), BF16),
                V((SHARE, C), BF16),
                V((SHARE + tokens, C), F32),
                V((tokens, C), F32),
                V((2, Z * SHARE, C), BF16),
                V((Z * SHARE, 2 * C), BF16),
                V((Z, SHARE, D), F32),
                V((4 * SHARE, rows), BF16),
                V((PIECES, half, 2 * CAP, piece), BF16),
                V((PIECES, half, 2 * CAP, piece), BF16),
                V((PIECES, 2, SHARE, piece), F32),
                V((PIECES, SHARE, piece), F32),
                DMA((8,)),
                DMA((Z,)),
                DMA((4,)),
                DMA((4,)),
                DMA((Z,)),
                DMA((Z,)),
                DMA((2, hops, PIECES)),
                DMA((2, hops, PIECES)),
                DMA((PIECES,)),
                DMA((PIECES,)),
                DMA((2,)),
                DMA((2,)),
                DMA((PIECES,)),
                DMA((PIECES,)),
                DMA((PIECES,)),
                DMA((PIECES,)),
            ],
            compiler_params=pltpu.CompilerParams(
                collective_id=0, has_side_effects=True, vmem_limit_bytes=60 * 1024 * 1024
            ),
            name="mixer_and_experts",
        )(
            mix_tokens,
            mix_gain.reshape(1, D),
            value_weight,
            inner_weight,
            outer_weight,
            conv_taps,
            mix_weight,
            moe_tokens,
            moe_gain.reshape(1, D),
            router_group.T,
            router_expert.T,
            expert_routes.T,
            gate_weight.reshape(D, F),
            up_weight.reshape(D, F),
            down_weight.reshape(F, D),
        )

    return jax.shard_map(
        local,
        mesh=mesh,
        in_specs=(
            P("ep", None),
            P(),
            P(None, "tp"),
            P(None, "tp"),
            P(None, "tp"),
            P(None, "tp"),
            P("tp", None),
            P("ep", None),
            P(),
            P(),
            P(),
            P("ep", None),
            P("ep", None, "tp"),
            P("ep", None, "tp"),
            P("ep", "tp", None),
        ),
        out_specs=(P(("ep", "tp"), None), P(("ep", "tp"), None)),
        check_vma=False,
    )
```

time: 128 us -> 91.8 us (0.72)
  Pallas kernels: 125 us -> 87.9 us
    pallas_call x1, Pallas kernels: 125 us -> 87.9 us  [local(): pl.pallas_call(functools.partial(kernel, EP, Z), out_shape=(out, out), in...]
where the time goes in v2:
time: 91.8 us; the launch traced here: 91.7 us
  Pallas kernels  87.9 us (96%)
  local copies, waits for them, and re-layouts  3.14 us (3%)
    pallas_call x1, Pallas kernels, local(): pl.pallas_call(functools.partial(kernel, EP, Z), out_shape=(out, out), in...  87.9 us
    unnamed x2, local copies, waits for them, and re-layouts  3.14 us

profile of v2, /device:TPU:3, one launch (start us, length us, event | category | flops | bytes accessed | tf_op | source)
XLA Modules:
  0.0 91.7 jit_solution(11642590224169067339)
XLA Ops:
  0.6 87.9 %mixer_and_experts.1 = (bf16[16,4096]{1,0:T(8,128)(2,1)}, bf16[16,4096]{1,0:T(8,128)(2,1)}) custom-call(bf16[256,4096]{1,0:T(8,128)(2,1)} %mix_x.1, f32[1,4096]{1,0:T(1,128)} %bitcast.13, bf16[4096,128]{1,0:T(8,128)(2,1)} %value_w.1, bf16[4096,128]{1,0:T(8,128)(2,1)} %inner_w.1, bf16[4096,128]{1,0:T(8,128)(2,1)} %outer_w.1, f32[3,128]{1,0:T(4,128)} %taps.1, ...), custom_call_target="tpu_custom_call" | custom-call | tf_op jit(solution)/shard_map/mixer_and_experts/pallas_call | solution.py:466
  88.5 1.6 %copy.19 = bf16[16,4096]{1,0:T(8,128)(2,1)} copy(bf16[16,4096]{1,0:T(8,128)(2,1)} %get-tuple-element.4) | data formatting | bytes 262144
  90.1 1.6 %copy.20 = bf16[16,4096]{1,0:T(8,128)(2,1)} copy(bf16[16,4096]{1,0:T(8,128)(2,1)} %get-tuple-element.5) | data formatting | bytes 262144

commit v3 on v2

--- a/solution.py
+++ b/solution.py
@@ -15,6 +15,10 @@
 EPG = 4
 EPS = 1e-06
 PIECES = 4
+WIDE = 2048
+LATER = 1
+VMEM_MIB = 60
+SIDE = 4
 AHEAD = 3
 
 
@@ -33,22 +37,28 @@
     EP,
     Z,
     mix_x,
-    mix_gain,
+    mix_gain_h,
     value_w,
     inner_w,
     outer_w,
-    taps,
+    taps_h,
     mix_w,
     moe_x,
-    moe_gain,
-    router_g,
-    router_e,
-    routes,
+    moe_gain_h,
+    router_g_h,
+    router_e_h,
+    routes_h,
     gate_w,
     up_w,
     down_w,
     mix_out,
     moe_out,
+    mix_gain,
+    taps,
+    moe_gain,
+    router_g,
+    router_e,
+    routes,
     raw_m,
     raw_e,
     norm_m,
@@ -62,6 +72,8 @@
     acc,
     rs_send,
     rs_recv,
+    mix_send,
+    mix_recv,
     halo_out,
     halo_in,
     gated,
@@ -76,14 +88,16 @@
     comb_in,
     load_sem,
     tok_sem,
+    small_sem,
     swap_send,
     swap_recv,
     disp_send,
     disp_recv,
+    credit,
     hop_send,
     hop_recv,
-    first_send,
-    first_recv,
+    mixhop_send,
+    mixhop_recv,
     halo_sem,
     conv_sem,
     back_send,
@@ -131,7 +145,19 @@
         span = pl.ds(pl.multiple_of(home_of(s) * home, home), home)
         return pltpu.make_async_copy(moe_x.at[span], raw_e.at[span], tok_sem.at[s])
 
-    token_load(0).start()
+    smalls = [
+        pltpu.make_async_copy(src, dst, small_sem.at[n])
+        for n, (src, dst) in enumerate(
+            [
+                (routes_h, routes),
+                (moe_gain_h, moe_gain),
+                (mix_gain_h, mix_gain),
+                (taps_h, taps),
+                (router_g_h, router_g),
+                (router_e_h, router_e),
+            ]
+        )
+    ]
     loads = [
         pltpu.make_async_copy(src, dst, load_sem.at[n])
         for n, (src, dst) in enumerate(
@@ -147,12 +173,16 @@
             ]
         )
     ]
+    smalls[0].start()
+    token_load(0).start()
+    smalls[1].start()
     barrier = pltpu.get_barrier_semaphore()
     greet = [to_expert(i) for i in range(half)] + [to_source(i) for i in range(half)]
     greet += [beside(1), beside(-1)]
     greet += [(lax.rem(e + 1, EP), tp), (lax.rem(e + EP - 1, EP), tp)]
     for device in greet:
         pl.semaphore_signal(barrier, inc=1, device_id=device, device_id_type=MESH)
+    smalls[2].start()
     for copy in loads[0:4]:
         copy.start()
 
@@ -161,7 +191,7 @@
         return carry
 
     lax.fori_loop(1, Z, load_tokens, 0)
-    for copy in loads[4:]:
+    for copy in loads[4:] + smalls[3:]:
         copy.start()
 
     row = lax.broadcasted_iota(jnp.int32, (rows, home), 0)
@@ -174,6 +204,7 @@
     before = ((bef_r < bef_c) & ((bef_r >> 4) == (bef_c >> 4))).astype(F32).astype(BF16)
     pick_r = lax.broadcasted_iota(jnp.int32, (tokens, home), 0)
     pick_c = lax.broadcasted_iota(jnp.int32, (tokens, home), 1)
+    smalls[0].wait()
     routes_b = routes[...].astype(F32).astype(BF16)
 
     def routed(zh):
@@ -186,8 +217,13 @@
         return h0, h1, at & is0, at & is1
 
     def dispatch(s):
-        for i in range(half):
-            remote(send.at[s, i], recv.at[s, slot], disp_send.at[s], disp_recv.at[s], to_expert(i)).start()
+        y, x = e // SIDE, lax.rem(e, SIDE)
+        odd = lax.rem(c + x, 2)
+        for dy in (2, 1, 3, 0):
+            for n in (0, 1):
+                dx = 2 - 2 * n + odd * (4 * n - 1)
+                i = (lax.rem(y + dy, SIDE) * SIDE + lax.rem(x + dx, SIDE)) // 2
+                remote(send.at[s, i], recv.at[s, slot], disp_send.at[s], disp_recv.at[s], to_expert(i)).start()
 
     def place(s):
         zh = home_of(s)
@@ -196,20 +232,10 @@
         start = pl.multiple_of(zh * home, home)
         token_load(s).wait()
         rms_rows(raw_e, moe_gain[...], norm_e, start, home)
-
-        def columns(n, carry):
-            cols = pl.ds(pl.multiple_of(n * 512, 512), 512)
+        for n in range(width // WIDE):
+            cols = slice(n * WIDE, (n + 1) * WIDE)
             placed = jnp.dot(chosen, norm_e[pl.ds(start, home), cols], preferred_element_type=F32)
-            send[s, :, :, cols] = placed.reshape(half, 2 * CAP, 512).astype(BF16)
-            return carry
-
-        lax.fori_loop(0, width // 512, columns, 0)
-
-        @pl.when(s == 0)
-        def _():
-            pl.semaphore_wait(barrier, len(greet))
-
-        dispatch(s)
+            send[s, :, :, cols] = placed.reshape(half, 2 * CAP, WIDE).astype(BF16)
 
     swaps = [
         remote(src, dst, swap_send.at[n], swap_recv.at[n], partner)
@@ -225,20 +251,26 @@
     halo = remote(halo_out, halo_in, halo_sem.at[0], halo_sem.at[1], (lax.rem(e + 1, EP), tp))
     conv_swap = remote(conv.at[1 - c], conv_all.at[:, C : 2 * C], conv_sem.at[0], conv_sem.at[1], partner)
 
-    def mixer_head():
+    def mixer_tail():
+        smalls[2].wait()
         loads[0].wait()
-        rms_rows(raw_m, mix_gain[...], norm_m, 0, tokens)
-        for n in (1, 2, 3):
+        rms_rows(raw_m, mix_gain[...], norm_m, tokens - SHARE, SHARE)
+        for n in (1, 2):
             loads[n].wait()
+        tail = jnp.dot(norm_m[tokens - SHARE :, :], proj_w[:, 0 : 2 * C], preferred_element_type=F32)
+        halo_out[...] = (tail[:, C:] * tail[:, 0:C]).astype(BF16)
+
+    def mixer_proj():
+        rms_rows(raw_m, mix_gain[...], norm_m, 0, tokens - SHARE)
+        loads[3].wait()
         proj = jnp.dot(norm_m[...], proj_w[...], preferred_element_type=F32)
         gated_in = (proj[:, C : 2 * C] * proj[:, 0:C]).astype(BF16)
         outer_p[...] = proj[:, 2 * C : 3 * C]
         gated[pl.ds(SHARE, tokens), :] = gated_in.astype(F32)
-        halo_out[...] = gated_in[tokens - SHARE :, :]
-        halo.start()
 
     def mixer_conv():
         halo.wait()
+        smalls[3].wait()
         gated[0:SHARE, :] = jnp.where(e > 0, halo_in[...].astype(F32), 0.0)
         mixed = taps[0:1, :] * gated[pl.ds(SHARE - 2, tokens), :]
         mixed = mixed + taps[1:2, :] * gated[pl.ds(SHARE - 1, tokens), :]
@@ -247,17 +279,40 @@
         conv[0] = conv_out[:, 0].reshape(Z * SHARE, C)
         conv[1] = conv_out[:, 1].reshape(Z * SHARE, C)
         conv_swap.start()
+        swaps[3].start()
         conv_all[:, 0:C] = conv[c]
 
-    def first_mix(j):
-        side = 1 if j < PIECES // 2 else 0
+    def mix_hop(direction, k):
+        if k == 0:
+            part = 1 - direction
+            src, dst = mix_send.at[direction, 0, part], mix_recv.at[direction, 0, part]
+        else:
+            src, dst = mix_send.at[direction, k], mix_recv.at[direction, k]
         return remote(
-            rs_send.at[side, 0, j, rows:],
-            rs_recv.at[side, 0, j, rows:],
-            first_send.at[j],
-            first_recv.at[j],
-            beside(2 * side - 1),
-        )
+            src, dst, mixhop_send.at[direction, k], mixhop_recv.at[direction, k], beside(2 * direction - 1)
+        )
+
+    def mixer_hop(k):
+        for direction in (1, 0):
+            zh = lax.rem(z + (2 * direction - 1) * (hops - k) + Z, Z)
+            if k:
+                mix_hop(direction, k - 1).wait_recv()
+            for part in (0, 1):
+                total = mix_part[zh, :, part * (width // 2) : (part + 1) * (width // 2)]
+                if k == 0 and part == direction:
+                    continue
+                if k > 1 or (k == 1 and part != direction):
+                    total = total + mix_recv[direction, k - 1, part].astype(F32)
+                mix_send[direction, k, part] = total.astype(BF16)
+            mix_hop(direction, k).start()
+
+    def mixer_end():
+        for direction in (1, 0):
+            mix_hop(direction, hops - 1).wait_recv()
+        for part in (0, 1):
+            cols = slice(part * (width // 2), (part + 1) * (width // 2))
+            total = mix_part[z, :, cols] + mix_recv[1, hops - 1, part].astype(F32)
+            mix_out[:, cols] = (total + mix_recv[0, hops - 1, part].astype(F32)).astype(BF16)
 
     def mixer_down():
         loads[4].wait()
@@ -271,13 +326,11 @@
             return carry
 
         lax.fori_loop(0, width // 512, down_mix, 0)
-        far = home_of(0)
-        for j in range(PIECES):
-            side = 1 if j < PIECES // 2 else 0
-            rs_send[side, 0, j, rows:, :] = mix_part[far, :, j * piece : (j + 1) * piece].astype(BF16)
-            first_mix(j).start()
+        mixer_hop(0)
 
     def weigh():
+        smalls[4].wait()
+        smalls[5].wait()
         h0, h1, at0, at1 = routed(z)
         own_normed = norm_e[pl.ds(pl.multiple_of(z * home, home), home), :]
         contract_last = (((1,), (1,)), ((), ()))
@@ -314,61 +367,71 @@
     def first_rows(j):
         side = 1 if j < PIECES // 2 else 0
         return remote(
-            rs_send.at[side, 0, j, 0:rows],
-            rs_recv.at[side, 0, j, 0:rows],
+            rs_send.at[side, 0, j],
+            rs_recv.at[side, 0, j],
             hop_send.at[side, 0, j],
             hop_recv.at[side, 0, j],
             beside(2 * side - 1),
         )
 
     def stage(s, carry):
-        @pl.when(s + AHEAD < Z)
+        @pl.when((s > 0) & (s - 1 + AHEAD < Z))
         def _():
-            place(s + AHEAD)
+            place(s - 1 + AHEAD)
+            pl.semaphore_wait(credit.at[s - 1], half)
+            dispatch(s - 1 + AHEAD)
 
         @pl.when(s == 0)
         def _():
-            mixer_conv()
+            mixer_down()
             for n in (5, 6, 7):
                 loads[n].wait()
             for n in (0, 1, 3):
                 swaps[n].wait_recv()
 
-        @pl.when(s == 1)
+        for k in range(1, hops):
+
+            @pl.when(s == (k if k < 3 else k + LATER))
+            def _():
+                mixer_hop(k)
+
+        @pl.when(s == Z - 1)
         def _():
-            mixer_down()
-
-        @pl.when(s == Z - AHEAD)
+            mixer_end()
+
+        @pl.when(s == Z + 1 - AHEAD)
         def _():
             weigh()
 
         arrived = remote(send.at[s], recv.at[s], disp_send.at[s], disp_recv.at[s], partner)
         arrived.wait_recv()
+
+        @pl.when(s + AHEAD < Z)
+        def _():
+            for i in range(half):
+                pl.semaphore_signal(credit.at[s], inc=1, device_id=to_source(i), device_id_type=MESH)
+
         x = recv[s].reshape(rows, width)
         gate_up = jnp.dot(x, gu_w[...], preferred_element_type=F32)
         g, u = gate_up[:, 0 : 2 * F], gate_up[:, 2 * F :]
         hidden = (g / (1.0 + jnp.exp(-g)) * u).astype(BF16)
         direction = lax.rem(s, 2)
         k = (s + 1) // 2
-        zs = home_of(s)
         for j in range(PIECES):
             cols = slice(j * piece, (j + 1) * piece)
             side = 1 if j < PIECES // 2 else 0
-            acc[0:rows, :] = jnp.dot(hidden, dn_w[:, cols], preferred_element_type=F32)
+            acc[...] = jnp.dot(hidden, dn_w[:, cols], preferred_element_type=F32)
 
             @pl.when(s == 0)
             def _():
-                rs_send[side, 0, j, 0:rows, :] = acc[0:rows, :].astype(BF16)
+                rs_send[side, 0, j] = acc[...].astype(BF16)
                 first_rows(j).start()
 
             @pl.when((s > 0) & (s < Z - 1))
             def _():
-                acc[rows:, :] = mix_part[zs, :, cols]
-
                 @pl.when((k == 1) & (direction == side))
                 def _():
                     first_rows(j).wait_recv()
-                    first_mix(j).wait_recv()
                     acc[...] += rs_recv[side, 0, j].astype(F32)
 
                 @pl.when(k > 1)
@@ -381,27 +444,32 @@
 
             @pl.when(s == Z - 1)
             def _():
-                acc[rows:, :] = mix_part[zs, :, cols]
                 for way in (1, 0):
                     hop(way, hops - 1, j).wait_recv()
                     acc[...] += rs_recv[way, hops - 1, j].astype(F32)
-                ret_send[j] = acc[0:rows, :].astype(BF16).reshape(half, 2 * CAP, piece)
+                ret_send[j] = acc[...].astype(BF16).reshape(half, 2 * CAP, piece)
                 for i in range(half):
                     give_back(j, i).start()
-                mix_out[:, cols] = acc[rows:, :].astype(BF16)
 
         return carry
 
+    smalls[1].wait()
     place(jnp.int32(0))
-    for copy in swaps:
-        copy.start()
-    mixer_head()
+    mixer_tail()
+    pl.semaphore_wait(barrier, len(greet))
+    halo.start()
+    dispatch(jnp.int32(0))
+    for n in (2, 0, 1):
+        swaps[n].start()
+    mixer_proj()
 
     def place_early(s, carry):
         place(s)
+        dispatch(s)
         return carry
 
     lax.fori_loop(1, AHEAD, place_early, 0)
+    mixer_conv()
     lax.fori_loop(0, Z, stage, 0)
 
     def last(j):
@@ -418,11 +486,13 @@
 
     for copy in swaps:
         copy.wait_send()
+    for k in range(hops):
+        for direction in (0, 1):
+            mix_hop(direction, k).wait_send()
     for s in range(Z):
         remote(send.at[s], recv.at[s], disp_send.at[s], disp_recv.at[s], partner).wait_send()
     for j in range(PIECES):
         first_rows(j).wait_send()
-        first_mix(j).wait_send()
         for k in range(1, hops):
             for direction in (0, 1):
                 hop(direction, k, j).wait_send()
@@ -459,16 +529,22 @@
         piece = D // PIECES
         hops = Z // 2
         vmem = pl.BlockSpec(memory_space=pltpu.VMEM)
-        hbm = pl.BlockSpec(memory_space=pl.ANY)
+        hbm = pl.BlockSpec(memory_space=pltpu.HBM)
         V = pltpu.VMEM
         DMA = pltpu.SemaphoreType.DMA
         out = jax.ShapeDtypeStruct((SHARE, D), BF16)
         return pl.pallas_call(
             functools.partial(kernel, EP, Z),
             out_shape=(out, out),
-            in_specs=[hbm, vmem, hbm, hbm, hbm, vmem, hbm, hbm, vmem, vmem, vmem, vmem, hbm, hbm, hbm],
+            in_specs=[hbm] * 15,
             out_specs=(vmem, vmem),
             scratch_shapes=[
+                V((1, D), F32),
+                V(conv_taps.shape, F32),
+                V((1, D), F32),
+                V((router_group.shape[1], D), BF16),
+                V((router_expert.shape[1], D), BF16),
+                V((2, tokens), jnp.int32),
                 V((tokens, D), BF16),
                 V((tokens, D), BF16),
                 V((tokens, D), BF16),
@@ -479,9 +555,11 @@
                 V((2 * C, D), BF16),
                 V((Z, half, 2 * CAP, D), BF16),
                 V((Z, half, 2 * CAP, D), BF16),
-                V((rows + SHARE, piece), F32),
-                V((2, hops, PIECES, rows + SHARE, piece), BF16),
-                V((2, hops, PIECES, rows + SHARE, piece), BF16),
+                V((rows, piece), F32),
+                V((2, hops, PIECES, rows, piece), BF16),
+                V((2, hops, PIECES, rows, piece), BF16),
+                V((2, hops, 2, SHARE, D // 2), BF16),
+                V((2, hops, 2, SHARE, D // 2), BF16),
                 V((SHARE, C), BF16),
                 V((SHARE, C), BF16),
                 V((SHARE + tokens, C), F32),
@@ -496,14 +574,16 @@
                 V((PIECES, SHARE, piece), F32),
                 DMA((8,)),
                 DMA((Z,)),
+                DMA((6,)),
                 DMA((4,)),
                 DMA((4,)),
                 DMA((Z,)),
                 DMA((Z,)),
+                pltpu.SemaphoreType.REGULAR((Z,)),
                 DMA((2, hops, PIECES)),
                 DMA((2, hops, PIECES)),
-                DMA((PIECES,)),
-                DMA((PIECES,)),
+                DMA((2, hops)),
+                DMA((2, hops)),
                 DMA((2,)),
                 DMA((2,)),
                 DMA((PIECES,)),
@@ -512,7 +592,7 @@
                 DMA((PIECES,)),
             ],
             compiler_params=pltpu.CompilerParams(
-                collective_id=0, has_side_effects=True, vmem_limit_bytes=60 * 1024 * 1024
+                collective_id=0, has_side_effects=True, vmem_limit_bytes=VMEM_MIB * 1024 * 1024
             ),
             name="mixer_and_experts",
         )(

time: 91.8 us -> 83 us (0.904); the launches traced: 91.7 us -> 81.9 us
  Pallas kernels: 87.9 us -> 78.1 us
    pallas_call x1, Pallas kernels: 87.9 us -> 78.1 us  [local(): pl.pallas_call(functools.partial(kernel, EP, Z), out_shape=(out, out), in...]
where the time goes in v3:
time: 83 us; the launch traced here: 81.9 us
  Pallas kernels  78.1 us (94%)
  local copies, waits for them, and re-layouts  3.14 us (4%)
    pallas_call x1, Pallas kernels, local(): pl.pallas_call(functools.partial(kernel, EP, Z), out_shape=(out, out), in...  78.1 us
    unnamed x2, local copies, waits for them, and re-layouts  3.14 us

profile of v3, /device:TPU:3, one launch (start us, length us, event | category | flops | bytes accessed | tf_op | source)
XLA Modules:
  0.0 81.9 jit_solution(14173397283654232880)
XLA Ops:
  0.6 78.1 %mixer_and_experts.1 = (bf16[16,4096]{1,0:T(8,128)(2,1)}, bf16[16,4096]{1,0:T(8,128)(2,1)}) custom-call(bf16[256,4096]{1,0:T(8,128)(2,1)} %mix_x.1, f32[1,4096]{1,0:T(1,128)} %bitcast.13, bf16[4096,128]{1,0:T(8,128)(2,1)} %value_w.1, bf16[4096,128]{1,0:T(8,128)(2,1)} %inner_w.1, bf16[4096,128]{1,0:T(8,128)(2,1)} %outer_w.1, f32[3,128]{1,0:T(4,128)} %taps_h.1, ...), custom_call_target="tpu_custom_call" | custom-call | tf_op jit(solution)/shard_map/mixer_and_experts/pallas_call | solution.py:536
  78.8 1.6 %copy.19 = bf16[16,4096]{1,0:T(8,128)(2,1)} copy(bf16[16,4096]{1,0:T(8,128)(2,1)} %get-tuple-element.4) | data formatting | bytes 262144
  80.3 1.6 %copy.20 = bf16[16,4096]{1,0:T(8,128)(2,1)} copy(bf16[16,4096]{1,0:T(8,128)(2,1)} %get-tuple-element.5) | data formatting | bytes 262144

commit v4 on v3

--- a/solution.py
+++ b/solution.py
@@ -16,7 +16,8 @@
 EPS = 1e-06
 PIECES = 4
 WIDE = 2048
-LATER = 1
+FINE = 1
+MIX_HOPS = ((0, 2, 1), (1, 1, 1), (0, 3, 2), (1, 2, 2), (1, 3, 5))
 VMEM_MIB = 60
 SIDE = 4
 AHEAD = 3
@@ -51,8 +52,7 @@
     gate_w,
     up_w,
     down_w,
-    mix_out,
-    moe_out,
+    out,
     mix_gain,
     taps,
     moe_gain,
@@ -86,6 +86,7 @@
     ret_recv,
     comb,
     comb_in,
+    out_v,
     load_sem,
     tok_sem,
     small_sem,
@@ -104,6 +105,7 @@
     back_recv,
     last_send,
     last_recv,
+    out_sem,
 ):
     tokens, width = raw_m.shape
     C = value_w.shape[1]
@@ -112,6 +114,8 @@
     rows = half * 2 * CAP
     piece = width // PIECES
     hops = Z // 2
+    fine = piece // FINE
+    parts = PIECES * FINE
 
     e = lax.axis_index("ep")
     tp = lax.axis_index("tp")
@@ -279,32 +283,32 @@
         conv[0] = conv_out[:, 0].reshape(Z * SHARE, C)
         conv[1] = conv_out[:, 1].reshape(Z * SHARE, C)
         conv_swap.start()
+        swaps[1].start()
         swaps[3].start()
         conv_all[:, 0:C] = conv[c]
 
     def mix_hop(direction, k):
-        if k == 0:
-            part = 1 - direction
-            src, dst = mix_send.at[direction, 0, part], mix_recv.at[direction, 0, part]
-        else:
-            src, dst = mix_send.at[direction, k], mix_recv.at[direction, k]
         return remote(
-            src, dst, mixhop_send.at[direction, k], mixhop_recv.at[direction, k], beside(2 * direction - 1)
-        )
-
-    def mixer_hop(k):
-        for direction in (1, 0):
-            zh = lax.rem(z + (2 * direction - 1) * (hops - k) + Z, Z)
-            if k:
-                mix_hop(direction, k - 1).wait_recv()
-            for part in (0, 1):
-                total = mix_part[zh, :, part * (width // 2) : (part + 1) * (width // 2)]
-                if k == 0 and part == direction:
-                    continue
-                if k > 1 or (k == 1 and part != direction):
-                    total = total + mix_recv[direction, k - 1, part].astype(F32)
-                mix_send[direction, k, part] = total.astype(BF16)
-            mix_hop(direction, k).start()
+            mix_send.at[direction, k],
+            mix_recv.at[direction, k],
+            mixhop_send.at[direction, k],
+            mixhop_recv.at[direction, k],
+            beside(2 * direction - 1),
+        )
+
+    def mixer_hop(direction, k):
+        zh = lax.rem(z + (2 * direction - 1) * (hops - k) + Z, Z)
+        came = k > 1 or (k == 1 and direction == 1)
+        if came:
+            mix_hop(direction, k - 1).wait_recv()
+        for part in (0, 1):
+            total = mix_part[zh, :, part * (width // 2) : (part + 1) * (width // 2)]
+            if came:
+                total = total + mix_recv[direction, k - 1, part].astype(F32)
+            mix_send[direction, k, part] = total.astype(BF16)
+        mix_hop(direction, k).start()
+
+    mix_write = pltpu.make_async_copy(out_v.at[0], out.at[0], out_sem.at[parts])
 
     def mixer_end():
         for direction in (1, 0):
@@ -312,21 +316,20 @@
         for part in (0, 1):
             cols = slice(part * (width // 2), (part + 1) * (width // 2))
             total = mix_part[z, :, cols] + mix_recv[1, hops - 1, part].astype(F32)
-            mix_out[:, cols] = (total + mix_recv[0, hops - 1, part].astype(F32)).astype(BF16)
+            out_v[0, :, cols] = (total + mix_recv[0, hops - 1, part].astype(F32)).astype(BF16)
+        mix_write.start()
 
     def mixer_down():
         loads[4].wait()
         swaps[2].wait_recv()
         conv_swap.wait()
 
-        def down_mix(n, carry):
-            cols = pl.ds(pl.multiple_of(n * 512, 512), 512)
+        for n in range(width // WIDE):
+            cols = slice(n * WIDE, (n + 1) * WIDE)
             part = jnp.dot(conv_all[...], mixw[:, cols], preferred_element_type=F32)
-            mix_part[:, :, cols] = part.reshape(Z, SHARE, 512)
-            return carry
-
-        lax.fori_loop(0, width // 512, down_mix, 0)
-        mixer_hop(0)
+            mix_part[:, :, cols] = part.reshape(Z, SHARE, WIDE)
+        mixer_hop(1, 0)
+        mixer_hop(0, 1)
 
     def weigh():
         smalls[4].wait()
@@ -352,29 +355,26 @@
         comb_w[0:home, :] = high
         comb_w[home : 2 * home, :] = (weight - high.astype(F32)).astype(BF16)
 
-    def hop(direction, k, j):
+    def hop(direction, k, j, h):
+        cols = slice(h * fine, (h + 1) * fine)
         return remote(
-            rs_send.at[direction, k, j],
-            rs_recv.at[direction, k, j],
-            hop_send.at[direction, k, j],
-            hop_recv.at[direction, k, j],
+            rs_send.at[direction, k, j, :, cols],
+            rs_recv.at[direction, k, j, :, cols],
+            hop_send.at[direction, k, j, h],
+            hop_recv.at[direction, k, j, h],
             beside(2 * direction - 1),
         )
 
-    def give_back(j, i):
-        return remote(ret_send.at[j, i], ret_recv.at[j, slot], back_send.at[j], back_recv.at[j], to_source(i))
-
-    def first_rows(j):
-        side = 1 if j < PIECES // 2 else 0
-        return remote(
-            rs_send.at[side, 0, j],
-            rs_recv.at[side, 0, j],
-            hop_send.at[side, 0, j],
-            hop_recv.at[side, 0, j],
-            beside(2 * side - 1),
-        )
+    def give_back(p, i):
+        return remote(ret_send.at[p, i], ret_recv.at[p, slot], back_send.at[p], back_recv.at[p], to_source(i))
 
     def stage(s, carry):
+        for direction, k, when in MIX_HOPS:
+
+            @pl.when(s == when)
+            def _():
+                mixer_hop(direction, k)
+
         @pl.when((s > 0) & (s - 1 + AHEAD < Z))
         def _():
             place(s - 1 + AHEAD)
@@ -383,17 +383,10 @@
 
         @pl.when(s == 0)
         def _():
-            mixer_down()
             for n in (5, 6, 7):
                 loads[n].wait()
             for n in (0, 1, 3):
                 swaps[n].wait_recv()
-
-        for k in range(1, hops):
-
-            @pl.when(s == (k if k < 3 else k + LATER))
-            def _():
-                mixer_hop(k)
 
         @pl.when(s == Z - 1)
         def _():
@@ -425,31 +418,39 @@
             @pl.when(s == 0)
             def _():
                 rs_send[side, 0, j] = acc[...].astype(BF16)
-                first_rows(j).start()
+                for h in range(FINE):
+                    hop(side, 0, j, h).start()
 
             @pl.when((s > 0) & (s < Z - 1))
             def _():
                 @pl.when((k == 1) & (direction == side))
                 def _():
-                    first_rows(j).wait_recv()
+                    for h in range(FINE):
+                        hop(side, 0, j, h).wait_recv()
                     acc[...] += rs_recv[side, 0, j].astype(F32)
 
                 @pl.when(k > 1)
                 def _():
-                    hop(direction, k - 1, j).wait_recv()
+                    for h in range(FINE):
+                        hop(direction, k - 1, j, h).wait_recv()
                     acc[...] += rs_recv[direction, k - 1, j].astype(F32)
 
                 rs_send[direction, k, j] = acc[...].astype(BF16)
-                hop(direction, k, j).start()
+                for h in range(FINE):
+                    hop(direction, k, j, h).start()
 
             @pl.when(s == Z - 1)
             def _():
-                for way in (1, 0):
-                    hop(way, hops - 1, j).wait_recv()
-                    acc[...] += rs_recv[way, hops - 1, j].astype(F32)
-                ret_send[j] = acc[...].astype(BF16).reshape(half, 2 * CAP, piece)
-                for i in range(half):
-                    give_back(j, i).start()
+                for h in range(FINE):
+                    span = slice(h * fine, (h + 1) * fine)
+                    for way in (1, 0):
+                        hop(way, hops - 1, j, h).wait_recv()
+                    total = acc[:, span] + rs_recv[1, hops - 1, j, :, span].astype(F32)
+                    total = total + rs_recv[0, hops - 1, j, :, span].astype(F32)
+                    p = j * FINE + h
+                    ret_send[p] = total.astype(BF16).reshape(half, 2 * CAP, fine)
+                    for i in range(half):
+                        give_back(p, i).start()
 
         return carry
 
@@ -459,45 +460,67 @@
     pl.semaphore_wait(barrier, len(greet))
     halo.start()
     dispatch(jnp.int32(0))
-    for n in (2, 0, 1):
+    for n in (2, 0):
         swaps[n].start()
     mixer_proj()
+    mixer_conv()
+    place(jnp.int32(1))
+    dispatch(jnp.int32(1))
+    mixer_down()
 
     def place_early(s, carry):
         place(s)
         dispatch(s)
         return carry
 
-    lax.fori_loop(1, AHEAD, place_early, 0)
-    mixer_conv()
+    lax.fori_loop(2, AHEAD, place_early, 0)
     lax.fori_loop(0, Z, stage, 0)
 
-    def last(j):
-        return remote(comb.at[j, 1 - c], comb_in.at[j], last_send.at[j], last_recv.at[j], partner)
-
-    for j in range(PIECES):
-        remote(ret_send.at[j], ret_recv.at[j], back_send.at[j], back_recv.at[j], partner).wait_recv()
-        summed = jnp.dot(comb_w[...], ret_recv[j].reshape(rows, piece), preferred_element_type=F32)
-        comb[j] = (summed[0:home] + summed[home:]).reshape(2, SHARE, piece)
-        last(j).start()
-    for j in range(PIECES):
-        last(j).wait_recv()
-        moe_out[:, j * piece : (j + 1) * piece] = (comb[j, c] + comb_in[j]).astype(BF16)
+    def last(p):
+        return remote(comb.at[p, 1 - c], comb_in.at[p], last_send.at[p], last_recv.at[p], partner)
+
+    def returned(p):
+        return remote(ret_send.at[p], ret_recv.at[p], back_send.at[p], back_recv.at[p], partner)
+
+    def finish(p):
+        last(p).wait_recv()
+        cols = slice(p * fine, (p + 1) * fine)
+        out_v[1, :, cols] = (comb[p, c] + comb_in[p]).astype(BF16)
+        write(p).start()
+
+    def write(p):
+        cols = slice(p * fine, (p + 1) * fine)
+        return pltpu.make_async_copy(out_v.at[1, :, cols], out.at[1, :, cols], out_sem.at[p])
+
+    for p in range(parts):
+        returned(p).wait_recv()
+        summed = jnp.dot(comb_w[...], ret_recv[p].reshape(rows, fine), preferred_element_type=F32)
+        comb[p] = (summed[0:home] + summed[home:]).reshape(2, SHARE, fine)
+        last(p).start()
+        if p > 1:
+            finish(p - 2)
+    for p in range(parts - 2, parts):
+        finish(p)
 
     for copy in swaps:
         copy.wait_send()
     for k in range(hops):
         for direction in (0, 1):
-            mix_hop(direction, k).wait_send()
+            if k or direction:
+                mix_hop(direction, k).wait_send()
     for s in range(Z):
         remote(send.at[s], recv.at[s], disp_send.at[s], disp_recv.at[s], partner).wait_send()
     for j in range(PIECES):
-        first_rows(j).wait_send()
-        for k in range(1, hops):
-            for direction in (0, 1):
-                hop(direction, k, j).wait_send()
-        remote(ret_send.at[j], ret_recv.at[j], back_send.at[j], back_recv.at[j], partner).wait_send()
-        last(j).wait_send()
+        for h in range(FINE):
+            hop(1 if j < PIECES // 2 else 0, 0, j, h).wait_send()
+            for k in range(1, hops):
+                for direction in (0, 1):
+                    hop(direction, k, j, h).wait_send()
+    for p in range(parts):
+        returned(p).wait_send()
+        last(p).wait_send()
+        write(p).wait()
+    mix_write.wait()
 
 
 def solution(mesh):
@@ -528,16 +551,16 @@
         rows = half * 2 * CAP
         piece = D // PIECES
         hops = Z // 2
-        vmem = pl.BlockSpec(memory_space=pltpu.VMEM)
-        hbm = pl.BlockSpec(memory_space=pltpu.HBM)
+        fine = piece // FINE
+        parts = PIECES * FINE
+        hbm = pl.BlockSpec(memory_space=pl.ANY)
         V = pltpu.VMEM
         DMA = pltpu.SemaphoreType.DMA
-        out = jax.ShapeDtypeStruct((SHARE, D), BF16)
-        return pl.pallas_call(
+        both = pl.pallas_call(
             functools.partial(kernel, EP, Z),
-            out_shape=(out, out),
+            out_shape=jax.ShapeDtypeStruct((2, SHARE, D), BF16),
             in_specs=[hbm] * 15,
-            out_specs=(vmem, vmem),
+            out_specs=hbm,
             scratch_shapes=[
                 V((1, D), F32),
                 V(conv_taps.shape, F32),
@@ -568,10 +591,11 @@
                 V((Z * SHARE, 2 * C), BF16),
                 V((Z, SHARE, D), F32),
                 V((4 * SHARE, rows), BF16),
-                V((PIECES, half, 2 * CAP, piece), BF16),
-                V((PIECES, half, 2 * CAP, piece), BF16),
-                V((PIECES, 2, SHARE, piece), F32),
-                V((PIECES, SHARE, piece), F32),
+                V((parts, half, 2 * CAP, fine), BF16),
+                V((parts, half, 2 * CAP, fine), BF16),
+                V((parts, 2, SHARE, fine), F32),
+                V((parts, SHARE, fine), F32),
+                V((2, SHARE, D), BF16),
                 DMA((8,)),
                 DMA((Z,)),
                 DMA((6,)),
@@ -580,16 +604,17 @@
                 DMA((Z,)),
                 DMA((Z,)),
                 pltpu.SemaphoreType.REGULAR((Z,)),
-                DMA((2, hops, PIECES)),
-                DMA((2, hops, PIECES)),
+                DMA((2, hops, PIECES, FINE)),
+                DMA((2, hops, PIECES, FINE)),
                 DMA((2, hops)),
                 DMA((2, hops)),
                 DMA((2,)),
                 DMA((2,)),
-                DMA((PIECES,)),
-                DMA((PIECES,)),
-                DMA((PIECES,)),
-                DMA((PIECES,)),
+                DMA((parts,)),
+                DMA((parts,)),
+                DMA((parts,)),
+                DMA((parts,)),
+                DMA((parts + 1,)),
             ],
             compiler_params=pltpu.CompilerParams(
                 collective_id=0, has_side_effects=True, vmem_limit_bytes=VMEM_MIB * 1024 * 1024
@@ -612,6 +637,7 @@
             up_weight.reshape(D, F),
             down_weight.reshape(F, D),
         )
+        return both[0], both[1]
 
     return jax.shard_map(
         local,

time: 83 us -> 81.4 us (0.981)
  local copies, waits for them, and re-layouts: 3.14 us -> 1.68 us
    unnamed x2 -> x0, local copies, waits for them, and re-layouts: 3.14 us -> none
    squeeze x0 -> x1, local copies, waits for them, and re-layouts: none -> 1.68 us  [local(): return (both[0], both[1])]
where the time goes in v4:
time: 81.4 us; the launch traced here: 80.2 us
  Pallas kernels  77.9 us (96%)
  local copies, waits for them, and re-layouts  1.68 us (2%)
    pallas_call x1, Pallas kernels, local(): pl.pallas_call(functools.partial(kernel, EP, Z), out_shape=jax.ShapeDtype...  77.9 us
    squeeze x1, local copies, waits for them, and re-layouts, local(): return (both[0], both[1])  1.68 us

profile of v4, /device:TPU:3, one launch (start us, length us, event | category | flops | bytes accessed | tf_op | source)
XLA Modules:
  0.0 80.2 jit_solution(5131911315422490601)
XLA Ops:
  0.6 77.9 %mixer_and_experts.1 = bf16[2,16,4096]{2,1,0:T(8,128)(2,1)} custom-call(bf16[256,4096]{1,0:T(8,128)(2,1)} %mix_x.1, f32[1,4096]{1,0:T(1,128)} %bitcast.17, bf16[4096,128]{1,0:T(8,128)(2,1)} %value_w.1, bf16[4096,128]{1,0:T(8,128)(2,1)} %inner_w.1, bf16[4096,128]{1,0:T(8,128)(2,1)} %outer_w.1, f32[3,128]{1,0:T(4,128)} %taps_h.1, bf16[128,4096]{1,0:T(8,128)(2,1)} %mix_w.1, ...), custom_call_target="tpu_custom_call" | custom-call | tf_op jit(solution)/shard_map/mixer_and_experts/pallas_call | solution.py:559
  78.5 1.7 %slice_bitcast_fusion = (bf16[16,4096]{1,0:T(8,128)(2,1)}, bf16[16,4096]{1,0:T(8,128)(2,1)}) fusion(bf16[2,16,4096]{2,1,0:T(8,128)(2,1)} %mixer_and_experts.1), kind=kLoop, calls=%fused_computation | loop fusion | bytes 524288 | tf_op jit(solution)/shard_map/squeeze | solution.py:640

commit v5 on v4

--- a/solution.py
+++ b/solution.py
@@ -16,8 +16,9 @@
 EPS = 1e-06
 PIECES = 4
 WIDE = 2048
+UNROLL = 3
 FINE = 1
-MIX_HOPS = ((0, 2, 1), (1, 1, 1), (0, 3, 2), (1, 2, 2), (1, 3, 5))
+MIX_HOPS = ((0, 2, 0), (1, 1, 0), (0, 3, 2), (1, 2, 2), (1, 3, 5))
 VMEM_MIB = 60
 SIDE = 4
 AHEAD = 3
@@ -31,7 +32,8 @@
         out[rows, :] = (values * inverse * gain).astype(BF16)
         return carry
 
-    lax.fori_loop(0, count // SHARE, body, 0)
+    trips = count // SHARE
+    lax.fori_loop(0, trips, body, 0, unroll=UNROLL if trips % UNROLL == 0 else 2 if trips % 2 == 0 else 1)
 
 
 def kernel(
@@ -227,7 +229,7 @@
             for n in (0, 1):
                 dx = 2 - 2 * n + odd * (4 * n - 1)
                 i = (lax.rem(y + dy, SIDE) * SIDE + lax.rem(x + dx, SIDE)) // 2
-                remote(send.at[s, i], recv.at[s, slot], disp_send.at[s], disp_recv.at[s], to_expert(i)).start()
+                remote(send.at[s, i], recv.at[s, slot], disp_send.at[0], disp_recv.at[s], to_expert(i)).start()
 
     def place(s):
         zh = home_of(s)
@@ -287,32 +289,31 @@
         swaps[3].start()
         conv_all[:, 0:C] = conv[c]
 
-    def mix_hop(direction, k):
+    def mix_hop(direction, k, part):
         return remote(
-            mix_send.at[direction, k],
-            mix_recv.at[direction, k],
-            mixhop_send.at[direction, k],
-            mixhop_recv.at[direction, k],
+            mix_send.at[direction, k, part],
+            mix_recv.at[direction, k, part],
+            mixhop_send.at[direction, min(k, 1)],
+            mixhop_recv.at[direction, k, part],
             beside(2 * direction - 1),
         )
 
     def mixer_hop(direction, k):
         zh = lax.rem(z + (2 * direction - 1) * (hops - k) + Z, Z)
-        came = k > 1 or (k == 1 and direction == 1)
-        if came:
-            mix_hop(direction, k - 1).wait_recv()
         for part in (0, 1):
             total = mix_part[zh, :, part * (width // 2) : (part + 1) * (width // 2)]
-            if came:
+            if k > 1 or (k == 1 and direction == 1):
+                mix_hop(direction, k - 1, part).wait_recv()
                 total = total + mix_recv[direction, k - 1, part].astype(F32)
             mix_send[direction, k, part] = total.astype(BF16)
-        mix_hop(direction, k).start()
-
-    mix_write = pltpu.make_async_copy(out_v.at[0], out.at[0], out_sem.at[parts])
+            mix_hop(direction, k, part).start()
+
+    mix_write = pltpu.make_async_copy(out_v.at[0], out.at[0], out_sem.at[0])
 
     def mixer_end():
         for direction in (1, 0):
-            mix_hop(direction, hops - 1).wait_recv()
+            for part in (0, 1):
+                mix_hop(direction, hops - 1, part).wait_recv()
         for part in (0, 1):
             cols = slice(part * (width // 2), (part + 1) * (width // 2))
             total = mix_part[z, :, cols] + mix_recv[1, hops - 1, part].astype(F32)
@@ -360,13 +361,13 @@
         return remote(
             rs_send.at[direction, k, j, :, cols],
             rs_recv.at[direction, k, j, :, cols],
-            hop_send.at[direction, k, j, h],
+            hop_send.at[direction, jnp.minimum(k, 1)],
             hop_recv.at[direction, k, j, h],
             beside(2 * direction - 1),
         )
 
     def give_back(p, i):
-        return remote(ret_send.at[p, i], ret_recv.at[p, slot], back_send.at[p], back_recv.at[p], to_source(i))
+        return remote(ret_send.at[p, i], ret_recv.at[p, slot], back_send.at[0], back_recv.at[p], to_source(i))
 
     def stage(s, carry):
         for direction, k, when in MIX_HOPS:
@@ -396,7 +397,7 @@
         def _():
             weigh()
 
-        arrived = remote(send.at[s], recv.at[s], disp_send.at[s], disp_recv.at[s], partner)
+        arrived = remote(send.at[s], recv.at[s], disp_send.at[0], disp_recv.at[s], partner)
         arrived.wait_recv()
 
         @pl.when(s + AHEAD < Z)
@@ -477,25 +478,27 @@
     lax.fori_loop(0, Z, stage, 0)
 
     def last(p):
-        return remote(comb.at[p, 1 - c], comb_in.at[p], last_send.at[p], last_recv.at[p], partner)
+        return remote(comb.at[1 - c, p], comb_in.at[p], last_send.at[0], last_recv.at[p], partner)
 
     def returned(p):
-        return remote(ret_send.at[p], ret_recv.at[p], back_send.at[p], back_recv.at[p], partner)
+        return remote(ret_send.at[p], ret_recv.at[p], back_send.at[0], back_recv.at[p], partner)
 
     def finish(p):
         last(p).wait_recv()
         cols = slice(p * fine, (p + 1) * fine)
-        out_v[1, :, cols] = (comb[p, c] + comb_in[p]).astype(BF16)
+        out_v[1, :, cols] = (comb[c, p] + comb_in[p]).astype(BF16)
         write(p).start()
 
     def write(p):
         cols = slice(p * fine, (p + 1) * fine)
-        return pltpu.make_async_copy(out_v.at[1, :, cols], out.at[1, :, cols], out_sem.at[p])
+        return pltpu.make_async_copy(out_v.at[1, :, cols], out.at[1, :, cols], out_sem.at[1])
 
     for p in range(parts):
         returned(p).wait_recv()
         summed = jnp.dot(comb_w[...], ret_recv[p].reshape(rows, fine), preferred_element_type=F32)
-        comb[p] = (summed[0:home] + summed[home:]).reshape(2, SHARE, fine)
+        summed = summed[0:home] + summed[home:]
+        comb[0, p] = summed[0:SHARE]
+        comb[1, p] = summed[SHARE:]
         last(p).start()
         if p > 1:
             finish(p - 2)
@@ -504,22 +507,23 @@
 
     for copy in swaps:
         copy.wait_send()
-    for k in range(hops):
-        for direction in (0, 1):
-            if k or direction:
-                mix_hop(direction, k).wait_send()
-    for s in range(Z):
-        remote(send.at[s], recv.at[s], disp_send.at[s], disp_recv.at[s], partner).wait_send()
-    for j in range(PIECES):
-        for h in range(FINE):
-            hop(1 if j < PIECES // 2 else 0, 0, j, h).wait_send()
-            for k in range(1, hops):
-                for direction in (0, 1):
-                    hop(direction, k, j, h).wait_send()
-    for p in range(parts):
-        returned(p).wait_send()
-        last(p).wait_send()
-        write(p).wait()
+    remote(mix_send.at[1, 0], mix_recv.at[1, 0], mixhop_send.at[1, 0], mixhop_recv.at[1, 0, 0], partner).wait_send()
+    remote(send, recv, disp_send.at[0], disp_recv.at[0], partner).wait_send()
+    for way in (0, 1):
+        later = pl.ds(1, hops - 1)
+        near = pl.ds((1 - way) * (PIECES // 2), PIECES // 2)
+        remote(
+            mix_send.at[way, later], mix_recv.at[way, later], mixhop_send.at[way, 1], mixhop_recv.at[way, 1, 0], partner
+        ).wait_send()
+        remote(
+            rs_send.at[way, 0, near], rs_recv.at[way, 0, near], hop_send.at[way, 0], hop_recv.at[way, 0, 0, 0], partner
+        ).wait_send()
+        remote(
+            rs_send.at[way, later], rs_recv.at[way, later], hop_send.at[way, 1], hop_recv.at[way, 1, 0, 0], partner
+        ).wait_send()
+    remote(ret_send, ret_recv, back_send.at[0], back_recv.at[0], partner).wait_send()
+    remote(comb.at[1 - c], comb_in, last_send.at[0], last_recv.at[0], partner).wait_send()
+    pltpu.make_async_copy(out_v.at[1], out.at[1], out_sem.at[1]).wait()
     mix_write.wait()
 
 
@@ -593,7 +597,7 @@
                 V((4 * SHARE, rows), BF16),
                 V((parts, half, 2 * CAP, fine), BF16),
                 V((parts, half, 2 * CAP, fine), BF16),
-                V((parts, 2, SHARE, fine), F32),
+                V((2, parts, SHARE, fine), F32),
                 V((parts, SHARE, fine), F32),
                 V((2, SHARE, D), BF16),
                 DMA((8,)),
@@ -601,20 +605,20 @@
                 DMA((6,)),
                 DMA((4,)),
                 DMA((4,)),
-                DMA((Z,)),
+                DMA((1,)),
                 DMA((Z,)),
                 pltpu.SemaphoreType.REGULAR((Z,)),
+                DMA((2, 2)),
                 DMA((2, hops, PIECES, FINE)),
-                DMA((2, hops, PIECES, FINE)),
-                DMA((2, hops)),
-                DMA((2, hops)),
+                DMA((2, 2)),
+                DMA((2, hops, 2)),
                 DMA((2,)),
                 DMA((2,)),
+                DMA((1,)),
                 DMA((parts,)),
+                DMA((1,)),
                 DMA((parts,)),
-                DMA((parts,)),
-                DMA((parts,)),
-                DMA((parts + 1,)),
+                DMA((2,)),
             ],
             compiler_params=pltpu.CompilerParams(
                 collective_id=0, has_side_effects=True, vmem_limit_bytes=VMEM_MIB * 1024 * 1024

time: 81.4 us -> 79.3 us (0.974); the launches traced: 80.2 us -> 79.2 us
  Pallas kernels: 77.9 us -> 76.9 us
    pallas_call x1, Pallas kernels: 77.9 us -> 76.9 us  [local(): pl.pallas_call(functools.partial(kernel, EP, Z), out_shape=jax.ShapeDtype...]
where the time goes in v5:
time: 79.3 us; the launch traced here: 79.2 us
  Pallas kernels  76.9 us (97%)
  local copies, waits for them, and re-layouts  1.68 us (2%)
    pallas_call x1, Pallas kernels, local(): pl.pallas_call(functools.partial(kernel, EP, Z), out_shape=jax.ShapeDtype...  76.9 us
    squeeze x1, local copies, waits for them, and re-layouts, local(): return (both[0], both[1])  1.68 us

profile of v5, /device:TPU:3, one launch (start us, length us, event | category | flops | bytes accessed | tf_op | source)
XLA Modules:
  0.0 79.2 jit_solution(6557609069105093969)
XLA Ops:
  0.6 76.9 %mixer_and_experts.1 = bf16[2,16,4096]{2,1,0:T(8,128)(2,1)} custom-call(bf16[256,4096]{1,0:T(8,128)(2,1)} %mix_x.1, f32[1,4096]{1,0:T(1,128)} %bitcast.17, bf16[4096,128]{1,0:T(8,128)(2,1)} %value_w.1, bf16[4096,128]{1,0:T(8,128)(2,1)} %inner_w.1, bf16[4096,128]{1,0:T(8,128)(2,1)} %outer_w.1, f32[3,128]{1,0:T(4,128)} %taps_h.1, bf16[128,4096]{1,0:T(8,128)(2,1)} %mix_w.1, ...), custom_call_target="tpu_custom_call" | custom-call | tf_op jit(solution)/shard_map/mixer_and_experts/pallas_call | solution.py:563
  77.5 1.7 %slice_bitcast_fusion = (bf16[16,4096]{1,0:T(8,128)(2,1)}, bf16[16,4096]{1,0:T(8,128)(2,1)}) fusion(bf16[2,16,4096]{2,1,0:T(8,128)(2,1)} %mixer_and_experts.1), kind=kLoop, calls=%fused_computation | loop fusion | bytes 524288 | tf_op jit(solution)/shard_map/squeeze | solution.py:644

commit v6 on v5

--- a/solution.py
+++ b/solution.py
@@ -378,7 +378,6 @@
 
         @pl.when((s > 0) & (s - 1 + AHEAD < Z))
         def _():
-            place(s - 1 + AHEAD)
             pl.semaphore_wait(credit.at[s - 1], half)
             dispatch(s - 1 + AHEAD)
 
@@ -452,6 +451,10 @@
                     ret_send[p] = total.astype(BF16).reshape(half, 2 * CAP, fine)
                     for i in range(half):
                         give_back(p, i).start()
+
+        @pl.when(s + AHEAD < Z)
+        def _():
+            place(s + AHEAD)
 
         return carry
 

time: 79.3 us -> 79.4 us (level)
  no operation moved by 1% of the time
where the time goes in v6:
time: 79.4 us; the launch traced here: 79.3 us
  Pallas kernels  77 us (97%)
  local copies, waits for them, and re-layouts  1.68 us (2%)
    pallas_call x1, Pallas kernels, local(): pl.pallas_call(functools.partial(kernel, EP, Z), out_shape=jax.ShapeDtype...  77 us
    squeeze x1, local copies, waits for them, and re-layouts, local(): return (both[0], both[1])  1.68 us

profile of v6, /device:TPU:3, one launch (start us, length us, event | category | flops | bytes accessed | tf_op | source)
XLA Modules:
  0.0 79.3 jit_solution(16916611950863586548)
XLA Ops:
  0.6 77.0 %mixer_and_experts.1 = bf16[2,16,4096]{2,1,0:T(8,128)(2,1)} custom-call(bf16[256,4096]{1,0:T(8,128)(2,1)} %mix_x.1, f32[1,4096]{1,0:T(1,128)} %bitcast.17, bf16[4096,128]{1,0:T(8,128)(2,1)} %value_w.1, bf16[4096,128]{1,0:T(8,128)(2,1)} %inner_w.1, bf16[4096,128]{1,0:T(8,128)(2,1)} %outer_w.1, f32[3,128]{1,0:T(4,128)} %taps_h.1, bf16[128,4096]{1,0:T(8,128)(2,1)} %mix_w.1, ...), custom_call_target="tpu_custom_call" | custom-call | tf_op jit(solution)/shard_map/mixer_and_experts/pallas_call | solution.py:566
  77.6 1.7 %slice_bitcast_fusion = (bf16[16,4096]{1,0:T(8,128)(2,1)}, bf16[16,4096]{1,0:T(8,128)(2,1)}) fusion(bf16[2,16,4096]{2,1,0:T(8,128)(2,1)} %mixer_and_experts.1), kind=kLoop, calls=%fused_computation | loop fusion | bytes 524288 | tf_op jit(solution)/shard_map/squeeze | solution.py:647
